TPU v7x, 512 devices: a whole 4x4x16 slice. The times are simulated.
512 devices in a mesh: kv: 64 (over z, y), tp: 8 (over x, core).
Axes of the slice: x: 4, y: 4, z: 16, core: 2. Of those that a mesh axis runs over, the one named last changes fastest.
Arguments:
- tokens: bfloat16 [4, 4, 4096], replicated, may hold values from -6 to 6
- parents: int32 [4, 4], replicated, may hold values from -1 to 2, as said below
- lengths: int32 [4], replicated, may hold values from 1 to 8184, as said below
- accepted: int32 [4], replicated, may hold values from 0 to 4
- in_gain: float32 [4096], replicated, may hold values from 0.1 to 1.9
- w_query: bfloat16 [4096, 3072], P('kv', 'tp'), may hold values from -0.09375 to 0.09375
- w_latent: bfloat16 [4096, 1024], P('kv'), may hold values from -0.09375 to 0.09375
- w_rope_key: bfloat16 [4096, 32], replicated, may hold values from -0.09375 to 0.09375
- latent_gain: float32 [1024], replicated, may hold values from 0.1 to 1.9
- query_gain: float32 [96], replicated, may hold values from 0.4 to 160, as said below
- key_gain: float32 [96], replicated, may hold values from 0.1 to 1.9
- w_key_up: bfloat16 [1024, 2048], P(None, 'tp'), may hold values from -0.1875 to 0.1875
- w_value_up: bfloat16 [1024, 2048], P(None, 'tp'), may hold values from -0.1875 to 0.1875
- w_out: bfloat16 [2048, 4096], P('tp', 'kv'), may hold values from -1 to 1
- out_gain: float32 [4096], P('kv'), may hold values from 0.1 to 1.9
- cache_latent: bfloat16 [4, 8192, 1024], P(None, 'kv'), may hold values from -6 to 6
- cache_rope: bfloat16 [4, 8192, 32], P(None, 'kv'), may hold values from -6 to 6
Outputs:
- mixed: bfloat16 [4, 4, 4096], P(None, None, 'kv')
- new_latent: bfloat16 [4, 8192, 1024], P(None, 'kv')
- new_rope: bfloat16 [4, 8192, 32], P(None, 'kv')
Inputs may be any that keep to these rules, and one draw needn't show every extreme that they name: parents[s, 0] is -1; for i of 1 or more parents[s, i] lies in 0 to i - 1. `lengths`: the first sequence's length is at most 8, the last one's at least 8056. `query_gain`: positive.
All inputs are finite; a program needn't handle non-finite values.
Results may differ from a plain program's by a relative error of at most 0.008.
The roundings to bfloat16 on the way count: a program that leaves them out, or rounds other values in their place, can miss the bound.
Values sent between devices are 32-bit elements; how exact they have to be, the bound alone decides.
No kernel may reach another device: no remote copies, remote signals or barrier semaphores. Data moves between devices by JAX's collectives and lax.ppermute only.
A program may use at most 64 MiB of HBM per device.

v0:
```python
import functools

import jax
import jax.numpy as jnp
import numpy as np
from jax import lax
from jax.experimental import pallas as pl
from jax.experimental.pallas import tpu as pltpu
from jax.sharding import Mesh
from jax.sharding import PartitionSpec as P


D = 4096
NOPE = 64
ROPE = 32
QK = 96
SEQS = 4
PROPS = 4
HEADS = 4
LANES = 128
EPS = 1e-06
KV = ("z", "y")
PLANE = ("y", "x", "c")
F32 = jnp.float32
BF16 = jnp.bfloat16
HIDDEN = -1e30

VMEM = pl.BlockSpec(memory_space=pltpu.VMEM)
HBM = pl.BlockSpec(memory_space=pltpu.HBM)
CHUNKS = 7
TURN_AT, SCALE_AT, VALUE_AT, WEIGHT_AT, BLOCK_ROWS = 256, 288, 296, 552, 680
ROPE_AT, COS_AT, A_AT, B_AT, SEEN_AT, ANCHOR_AT = 0, 4, 8, 12, 16, 32
QN_AT, QR_AT, KN_AT, KR_AT, OUT_AT, START_AT, LATENT_AT = 33, 34, 35, 36, 37, 38, 40
GAIN_AT, TABLE_ROWS = 48, 144
WINDOW = 32


def kernel(body, outs, *args, specs=None, out_specs=None, scratch=(), aliases=None, mebibytes=8):
    shapes = [jax.ShapeDtypeStruct(shape, kind) for shape, kind in outs]
    out_specs = list(out_specs) if out_specs else [VMEM] * len(shapes)
    single = len(shapes) == 1
    return pl.pallas_call(
        body,
        out_shape=shapes[0] if single else shapes,
        in_specs=list(specs) if specs else [VMEM] * len(args),
        out_specs=out_specs[0] if single else out_specs,
        scratch_shapes=list(scratch),
        input_output_aliases=aliases or {},
        cost_estimate=pl.CostEstimate(flops=2_000_000, bytes_accessed=1_000_000, transcendentals=0),
        compiler_params=pltpu.CompilerParams(vmem_limit_bytes=mebibytes * 2**20),
    )(*args)


def lanes_of(shape):
    return lax.broadcasted_iota(jnp.int32, shape, len(shape) - 1)


def rows_of(shape):
    return lax.broadcasted_iota(jnp.int32, shape, len(shape) - 2)


def matmul(left, right):
    return lax.dot_general(left, right, (((1,), (0,)), ((), ())), preferred_element_type=F32)


def matmul_t(left, right):
    return lax.dot_general(left, right, (((1,), (1,)), ((), ())), preferred_element_type=F32)


def half_pick(low, high):
    shape = jnp.broadcast_shapes(low.shape, high.shape)
    shape = (*shape[:-1], LANES)
    return jnp.where(lanes_of(shape) < NOPE, low, high)


def quarter_pick(parts):
    shape = (*parts[0].shape[:-1], LANES)
    lane = lanes_of(shape)
    return jnp.where(
        lane < NOPE,
        jnp.where(lane < ROPE, parts[0], parts[1]),
        jnp.where(lane < NOPE + ROPE, parts[2], parts[3]),
    )


def head_scales(first, second, rope_squares):
    lane = lanes_of(first.shape)
    found = []
    for h, part in enumerate((first, first, second, second)):
        inside = lane < NOPE if h % 2 == 0 else lane >= NOPE
        squares = jnp.sum(jnp.where(inside, part * part, 0.0), -1, keepdims=True)
        found.append(lax.rsqrt((squares + rope_squares[h]) / QK + EPS))
    return found


def gains(gain_row):
    nope = gain_row[:, :NOPE]
    rope = gain_row[:, NOPE:QK]
    return jnp.concatenate([nope, nope], 1), jnp.concatenate([rope] * 4, 1)


def keys_of(nope, rope_tiled, nope_gain, rope_gain):
    first, second = nope[:, :LANES], nope[:, LANES:]
    lane = lanes_of(rope_tiled.shape)
    rope_sum = jnp.sum(jnp.where(lane < ROPE, rope_tiled * rope_tiled, 0.0), -1, keepdims=True)
    scales = head_scales(first, second, [rope_sum] * 4)
    return (
        first * half_pick(scales[0], scales[1]) * nope_gain,
        second * half_pick(scales[2], scales[3]) * nope_gain,
        rope_tiled * quarter_pick(scales) * rope_gain,
    )


def attend(products, values, seen):
    scale = QK ** (-0.5)
    scores = [jnp.where(v, p * scale, HIDDEN) for p, v in zip(products, seen)]
    peak = functools.reduce(jnp.maximum, [jnp.max(s, -1, keepdims=True) for s in scores])
    weights = [jnp.where(v, jnp.exp(s - peak), 0.0) for s, v in zip(scores, seen)]
    total = sum(jnp.sum(w, -1, keepdims=True) for w in weights)
    sums = [0.0, 0.0]
    for weight, value in zip(weights, values):
        low = weight.astype(BF16)
        for j, part in enumerate(value):
            high_part = part.astype(BF16)
            rest = (part - high_part.astype(F32)).astype(BF16)
            sums[j] = sums[j] + matmul(low, high_part) + matmul(low, rest)
    first = half_pick(sums[0][0:4], sums[0][4:8])
    second = half_pick(sums[1][8:12], sums[1][12:16])
    lane = lanes_of((PROPS, LANES))
    stats = jnp.zeros((PROPS, LANES), F32)
    for h in range(HEADS):
        stats = jnp.where(lane == h, peak[4 * h : 4 * h + 4], stats)
        stats = jnp.where(lane == HEADS + h, total[4 * h : 4 * h + 4], stats)
    return first, second, stats


def sine_cosine(angle):
    turns = jnp.floor(angle * (2.0 / np.pi) + 0.5)
    rest = ((angle - turns * 1.5703125) - turns * 4.837512969970703125e-4) - turns * 7.549789954891882e-8
    square = rest * rest
    sine = rest + rest * square * (
        -1.6666654611e-1 + square * (8.3321608736e-3 + square * -1.9515295891e-4)
    )
    cosine = (
        1.0
        - 0.5 * square
        + square
        * square
        * (4.166664568298827e-2 + square * (-1.388731625493765e-3 + square * 2.443315711809948e-5))
    )
    quadrant = turns - 4.0 * jnp.floor(turns * 0.25)
    odd = (quadrant == 1.0) | (quadrant == 3.0)
    sine_out = jnp.where(odd, cosine, sine)
    cosine_out = jnp.where(odd, sine, cosine)
    sine_out = jnp.where(quadrant >= 2.0, -sine_out, sine_out)
    cosine_out = jnp.where((quadrant == 1.0) | (quadrant == 2.0), -cosine_out, cosine_out)
    return sine_out, cosine_out


def turn(rope_tiled, cosine, sine_a, sine_b):
    return (
        rope_tiled * cosine
        + pltpu.roll(rope_tiled, LANES - 16, 1) * sine_a
        + pltpu.roll(rope_tiled, 16, 1) * sine_b
    )


def ancestors(parents_ref, s):
    masks = []
    for i in range(PROPS):
        mask = jnp.int32(1 << i)
        if i:
            parent = parents_ref[s, i]
            for j in range(i):
                mask = mask + jnp.where(parent == j, masks[j], 0)
        masks.append(mask)
    return masks


def bits(mask):
    return sum((mask >> j) & 1 for j in range(PROPS))


def start_body(
    parents_hbm,
    lengths_hbm,
    accepted_hbm,
    tok_hbm,
    gain_hbm,
    wq_hbm,
    wl_hbm,
    wr_hbm,
    inverse_hbm,
    lgain_hbm,
    qgain_hbm,
    kgain_hbm,
    ogain_hbm,
    wo_hbm,
    rope_hbm,
    wk_hbm,
    wv_hbm,
    cache_hbm,
    out_ref,
    block_0,
    block_1,
    block_2,
    block_3,
    table_ref,
    window_ref,
    rope_out_ref,
    copy_hbm,
    parents_ref,
    lengths_ref,
    accepted_ref,
    tok_ref,
    gain_ref,
    wq_ref,
    wl_ref,
    wr_ref,
    inverse_ref,
    lgain_ref,
    qgain_ref,
    kgain_ref,
    ogain_ref,
    wo_ref,
    rope_ref,
    wk_ref,
    wv_ref,
    cache_ref,
    sems,
):
    sources = (
        parents_hbm, lengths_hbm, accepted_hbm, tok_hbm, gain_hbm, wq_hbm, wl_hbm, wr_hbm, inverse_hbm,
        lgain_hbm, qgain_hbm, kgain_hbm, ogain_hbm, wo_hbm, rope_hbm, wk_hbm, wv_hbm, cache_hbm,
    )
    targets = (
        parents_ref, lengths_ref, accepted_ref, tok_ref, gain_ref, wq_ref, wl_ref, wr_ref, inverse_ref,
        lgain_ref, qgain_ref, kgain_ref, ogain_ref, wo_ref, rope_ref, wk_ref, wv_ref, cache_ref,
    )
    copies = [pltpu.make_async_copy(a, b, sems.at[k]) for k, (a, b) in enumerate(zip(sources, targets))]
    for copy in copies:
        copy.start()
    for copy in copies[:-4]:
        copy.wait()
    y = lax.axis_index("y")
    kv = lax.axis_index("z") * lax.axis_size("y") + y
    rows = wq_ref.shape[0]
    width = max(rows, LANES)
    per = width // rows
    base = pl.multiple_of((kv // per) * width, LANES)
    positions = cache_ref.shape[1]

    parts, normed = [], []
    for s in range(SEQS):
        tok = tok_ref[s].astype(F32)
        scale = lax.rsqrt(jnp.sum(tok * tok, -1, keepdims=True) / D + EPS)
        normed.append(tok * scale * gain_ref[...])
        piece = tok_ref[s, :, pl.ds(base, width)].astype(F32)
        parts.append(piece * scale * gain_ref[:, pl.ds(base, width)])
    part = jnp.concatenate(parts, 0)
    if per > 1:
        part = jnp.where(lanes_of(part.shape) // rows == kv % per, part, 0.0)
    part = part.astype(BF16)
    half = wl_ref.shape[1] // 2
    wl = wl_ref[:, pl.ds(pl.multiple_of(lax.axis_index("c") * half, LANES), half)]
    query = matmul(part, jnp.concatenate([wq_ref[...]] * per, 0))
    latent = matmul(part, jnp.concatenate([wl] * per, 0))
    nope = [query[:, QK * h : QK * h + NOPE] for h in range(HEADS)]
    rope = [query[:, QK * h + NOPE : QK * h + QK] for h in range(HEADS)]
    chunks = [
        jnp.concatenate(nope[:2], 1),
        jnp.concatenate(nope[2:], 1),
        jnp.concatenate(rope, 1),
    ] + [latent[:, LANES * k : LANES * k + LANES] for k in range(half // LANES)]
    for s in range(SEQS):
        for k, chunk in enumerate(chunks):
            out_ref[s, k] = chunk[4 * s : 4 * s + 4]

    row = rows_of((16, LANES))
    place = jnp.zeros((16, LANES), F32)
    starts = []
    for s in range(SEQS):
        anchor = lengths_ref[s] + accepted_ref[s]
        starts.append(anchor - kv * positions)
        for i, mask in enumerate(ancestors(parents_ref, s)):
            place = jnp.where(row == 4 * s + i, (anchor + bits(mask) - 1).astype(F32), place)
    raw = matmul_t(jnp.concatenate(normed, 0).astype(BF16), wr_ref[...])
    raw = jnp.concatenate([raw] * 4, 1)
    sine, cosine = sine_cosine(place * inverse_ref[...])
    early = lanes_of((16, LANES)) % ROPE < 16
    sine_a = jnp.where(early, -sine, 0.0)
    sine_b = jnp.where(early, 0.0, sine)
    fresh = turn(raw, cosine, sine_a, sine_b)
    for at, full in ((ROPE_AT, fresh), (COS_AT, cosine), (A_AT, sine_a), (B_AT, sine_b)):
        own = full[0:4]
        for s in range(1, SEQS):
            own = jnp.where(y == s, full[4 * s : 4 * s + 4], own)
        table_ref[at : at + 4] = own
    masks = ancestors(parents_ref, y)
    prop, lane = row % PROPS, lanes_of((16, LANES))
    seen = jnp.zeros((16, LANES), jnp.int32)
    for i in range(PROPS):
        for j in range(i + 1):
            seen = jnp.where((prop == i) & (lane == j), (masks[i] >> j) & 1, seen)
    table_ref[SEEN_AT : SEEN_AT + 16] = seen.astype(F32)
    anchor = (lengths_ref[y] + accepted_ref[y]).astype(F32)
    table_ref[ANCHOR_AT : ANCHOR_AT + 1] = jnp.zeros((1, LANES), F32) + anchor
    nope_gain, rope_gain = gains(kgain_ref[...])
    table_ref[KN_AT : KN_AT + 1], table_ref[KR_AT : KR_AT + 1] = nope_gain, rope_gain
    table_ref[QN_AT : QN_AT + 1], table_ref[QR_AT : QR_AT + 1] = gains(qgain_ref[...])
    table_ref[OUT_AT : OUT_AT + 1] = jnp.concatenate([ogain_ref[...]] * (LANES // ogain_ref.shape[1]), 1)
    spot = lanes_of((2, LANES))
    begun = jnp.zeros((2, LANES), F32)
    for s in range(SEQS):
        begun = jnp.where(spot == s, starts[s].astype(F32), begun)
    table_ref[START_AT : START_AT + 2] = begun
    for k in range(8):
        table_ref[LATENT_AT + k : LATENT_AT + k + 1] = lgain_ref[:, LANES * k : LANES * k + LANES]
    tall_gain = jnp.concatenate([nope_gain, rope_gain, jnp.zeros((6, LANES), F32)], 0)
    tall_gain = jnp.concatenate([tall_gain] * (LANES // 8), 0).T
    table_ref[GAIN_AT : GAIN_AT + NOPE] = jnp.zeros((NOPE, LANES), F32) + tall_gain[:NOPE, 0:1]
    table_ref[GAIN_AT + NOPE : GAIN_AT + QK] = jnp.zeros((ROPE, LANES), F32) + tall_gain[:ROPE, 1:2]
    flipped = jnp.concatenate([fresh, jnp.zeros((LANES - 16, LANES), F32)], 0).T[:ROPE]

    for copy in copies[-4:]:
        copy.wait()
    kept = pltpu.make_async_copy(cache_ref, copy_hbm, sems.at[len(copies)])
    kept.start()
    weights = wo_ref[...].astype(F32)
    for k, block_ref in enumerate((block_0, block_1, block_2, block_3)):
        s = lax.rem(y + k, SEQS)
        block = cache_ref[s]
        nope = matmul(block, wk_ref[...])
        value = matmul(block, wv_ref[...])
        old = rope_ref[s].astype(F32)
        old_sum = jnp.sum(old * old, 0, keepdims=True)
        block_ref[TURN_AT : TURN_AT + ROPE] = old
        for j in range(2):
            flat = nope[:, LANES * j : LANES * j + LANES].T
            block_ref[LANES * j : LANES * j + LANES] = flat
            block_ref[VALUE_AT + LANES * j : VALUE_AT + LANES * j + LANES] = value[:, LANES * j : LANES * j + LANES]
            for i in range(2):
                dims = flat[NOPE * i : NOPE * i + NOPE]
                squares = jnp.sum(dims * dims, 0, keepdims=True) + old_sum
                h = SCALE_AT + 2 * j + i
                block_ref[h : h + 1] = lax.rsqrt(squares / QK + EPS)
        block_ref[SCALE_AT + 4 : SCALE_AT + 8] = jnp.zeros((4, LANES), F32)
        block_ref[WEIGHT_AT : WEIGHT_AT + 64] = weights[:, :LANES]
        block_ref[WEIGHT_AT + 64 : WEIGHT_AT + 128] = weights[:, LANES:]
    for s in range(SEQS):
        old = rope_ref[s].astype(F32)
        spot = lanes_of(old.shape)
        for p in range(PROPS):
            old = jnp.where(spot == starts[s] + p, flipped[:, 4 * s + p : 4 * s + p + 1], old)
        rope_out_ref[s] = old.astype(BF16)
        window_ref[s] = cache_ref[s, pl.ds(window_base(starts[s], positions), WINDOW), :]
    kept.wait()


def window_base(start, positions):
    return pl.multiple_of(jnp.clip(start // 16, 0, positions // 16 - WINDOW // 16) * 16, 16)


def relay_body(in_ref, out_ref):
    total = in_ref[0]
    for k in range(1, in_ref.shape[0]):
        total = total + in_ref[k]
    for k in range(out_ref.shape[0]):
        out_ref[k] = total


def query_body(in_ref, table_ref, query_ref, latent_ref):
    total = in_ref[0]
    for k in range(1, in_ref.shape[0]):
        total = total + in_ref[k]
    first, second = total[0], total[1]
    rope = turn(
        total[2],
        table_ref[COS_AT : COS_AT + 4],
        table_ref[A_AT : A_AT + 4],
        table_ref[B_AT : B_AT + 4],
    )
    lane = lanes_of(rope.shape)
    sums = [
        jnp.sum(jnp.where(lane // ROPE == h, rope * rope, 0.0), -1, keepdims=True)
        for h in range(HEADS)
    ]
    scales = head_scales(first, second, sums)
    nope_gain, rope_gain = table_ref[QN_AT : QN_AT + 1], table_ref[QR_AT : QR_AT + 1]
    first = first * half_pick(scales[0], scales[1]) * nope_gain
    second = second * half_pick(scales[2], scales[3]) * nope_gain
    rope = rope * quarter_pick(scales) * rope_gain
    for h in range(HEADS):
        inside = (lane < NOPE) if h % 2 == 0 else (lane >= NOPE)
        empty = jnp.zeros_like(first)
        query_ref[0, 4 * h : 4 * h + 4] = jnp.where(inside, first, 0.0) if h < 2 else empty
        query_ref[1, 4 * h : 4 * h + 4] = jnp.where(inside, second, 0.0) if h >= 2 else empty
        query_ref[2, 4 * h : 4 * h + 4] = jnp.where(lane // ROPE == h, rope, 0.0)
    latent_ref[...] = total[3:CHUNKS]


def attend_body(latent_ref, table_ref, query_ref, wk_ref, wv_ref, *refs):
    block_refs, (out_ref, own_ref, fresh_ref) = refs[:SEQS], refs[SEQS:]
    query = [query_ref[j].astype(BF16) for j in range(3)]
    pieces = [latent_ref[c, k] for c in range(2) for k in range(4)]
    squares = sum(jnp.sum(piece * piece, -1, keepdims=True) for piece in pieces)
    scale = lax.rsqrt(squares / (8 * LANES) + EPS)
    pieces = [p * scale * table_ref[LATENT_AT + k : LATENT_AT + k + 1] for k, p in enumerate(pieces)]
    for k, piece in enumerate(pieces):
        fresh_ref[k] = piece
    fresh = jnp.concatenate(pieces, 1)
    low = jnp.concatenate([fresh, jnp.zeros_like(fresh)], 0).astype(BF16)
    value = matmul(low, wv_ref[...])
    rope = table_ref[ROPE_AT : ROPE_AT + 4].astype(BF16).astype(F32)
    tiled = jnp.concatenate([rope, jnp.zeros_like(rope)], 0)
    key = keys_of(
        matmul(low, wk_ref[...]), tiled, table_ref[KN_AT : KN_AT + 1], table_ref[KR_AT : KR_AT + 1]
    )
    pad = jnp.zeros((LANES - 8, LANES), F32)
    key = [jnp.concatenate([k, pad], 0).astype(BF16) for k in key]
    value = [jnp.concatenate([v, pad], 0) for v in (value[:, :LANES], value[:, LANES:])]
    own = sum(matmul_t(q, k) for q, k in zip(query, key))
    for j, part in enumerate(attend([own], [value], [table_ref[SEEN_AT : SEEN_AT + 16] > 0.5])):
        own_ref[j] = part
    anchor = table_ref[ANCHOR_AT : ANCHOR_AT + 1]
    nope_gain = table_ref[GAIN_AT : GAIN_AT + NOPE]
    rope_gain = table_ref[GAIN_AT + NOPE : GAIN_AT + QK]
    products, values, seen = [], [], []
    for k, block_ref in enumerate(block_refs):
        source = lax.rem(lax.axis_index("y") + SEQS - k, SEQS)
        start = (lax.axis_index("z") * SEQS + source) * LANES
        scales = [block_ref[SCALE_AT + h : SCALE_AT + h + 1] for h in range(HEADS)]
        rope = block_ref[TURN_AT : TURN_AT + ROPE]
        keys = [
            block_ref[NOPE * h : NOPE * h + NOPE] * scales[h] * nope_gain for h in range(HEADS)
        ] + [rope * scales[h] * rope_gain for h in range(HEADS)]
        key = jnp.concatenate(keys, 0).astype(BF16)
        products.append(sum(matmul(q, key[LANES * j : LANES * j + LANES]) for j, q in enumerate(query)))
        values.append([block_ref[VALUE_AT + LANES * j : VALUE_AT + LANES * j + LANES] for j in range(2)])
        seen.append((lanes_of((16, LANES)) + start).astype(F32) < anchor)
    packed = attend(products, values, seen)
    for k in range(out_ref.shape[0]):
        for j, part in enumerate(packed):
            out_ref[k, j] = part


def merge_body(in_ref, own_ref, fresh_ref, *refs):
    block_refs, out_ref = refs[:-1], refs[-1]
    y = lax.axis_index("y")
    share = lax.axis_index("x") * lax.axis_size("c") + lax.axis_index("c")
    parts = [[in_ref[k, j] for j in range(3)] for k in range(in_ref.shape[0])]
    parts.append([own_ref[j] for j in range(3)])
    peak = functools.reduce(jnp.maximum, [stats for _, _, stats in parts])
    first = second = total = 0.0
    for first_part, second_part, stats in parts:
        scale = jnp.exp(stats - peak)
        total = total + pltpu.roll(stats, LANES - HEADS, 1) * scale
        first = first + first_part * half_pick(scale[:, 0:1], scale[:, 1:2])
        second = second + second_part * half_pick(scale[:, 2:3], scale[:, 3:4])
    first = first / half_pick(total[:, 0:1], total[:, 1:2])
    second = second / half_pick(total[:, 2:3], total[:, 3:4])
    pad = jnp.zeros((4, LANES), F32)
    first = jnp.concatenate([first, pad], 0).astype(BF16)
    second = jnp.concatenate([second, pad], 0).astype(BF16)
    sums = [jnp.zeros((8, LANES), F32) for _ in range(SEQS)]
    for k, block_ref in enumerate(block_refs):
        weight = block_ref[WEIGHT_AT : WEIGHT_AT + LANES].astype(BF16)
        low = matmul_t(first, weight) + pltpu.roll(matmul_t(second, weight), NOPE, 1)
        both = half_pick(low, pltpu.roll(low, NOPE, 1))
        place = lax.rem(y + SEQS - k, SEQS)
        sums = [jnp.where(place == j, both, sums[j]) for j in range(SEQS)]
    packed = (half_pick(sums[0], sums[1])[0:4], half_pick(sums[2], sums[3])[0:4], fresh_ref[share])
    for k in range(out_ref.shape[0]):
        for j, part in enumerate(packed):
            out_ref[k, j] = part


def gather_body(in_ref, own_ref, square_ref, latent_ref):
    y = lax.axis_index("y")
    peers = in_ref.shape[0] // SEQS
    lane = lanes_of((PROPS, LANES))
    squares = jnp.zeros((PROPS, LANES), F32)
    for s in range(SEQS):
        first, second = in_ref[peers * s, 0], in_ref[peers * s, 1]
        for t in range(1, peers):
            first = first + in_ref[peers * s + t, 0]
            second = second + in_ref[peers * s + t, 1]
        square = jnp.sum(first * first + second * second, -1, keepdims=True)
        squares = jnp.where(lane == s, square, squares)
        picked = jnp.where(y < 2, first, second)
        own_ref[s] = jnp.where(lax.rem(y, 2) == 0, picked, pltpu.roll(picked, NOPE, 1))
        for t in range(peers):
            latent_ref[s, :, LANES * t : LANES * t + LANES] = in_ref[peers * s + t, 2]
    for k in range(square_ref.shape[0]):
        square_ref[k] = squares


def finish_body(in_ref, own_ref, table_ref, window_ref, fresh_ref, copy_hbm, mixed_ref, out_hbm, patch_ref, sems):
    del copy_hbm
    positions = out_hbm.shape[1]
    begun = table_ref[START_AT : START_AT + 1]
    lane = lanes_of(begun.shape)
    starts = [jnp.sum(jnp.where(lane == s, begun, 0.0)).astype(jnp.int32) for s in range(SEQS)]
    for s, start in enumerate(starts):

        @pl.when((start > -PROPS) & (start < positions))
        def _(s=s, start=start):
            base = window_base(start, positions)
            window = window_ref[s].astype(F32)
            row = rows_of(window.shape) + base
            for p in range(PROPS):
                window = jnp.where(row == start + p, fresh_ref[s, p : p + 1, :], window)
            patch_ref[s] = window.astype(BF16)
            pltpu.make_async_copy(patch_ref.at[s], out_hbm.at[s, pl.ds(base, WINDOW), :], sems.at[s]).start()

    total = in_ref[0]
    for k in range(1, in_ref.shape[0]):
        total = total + in_ref[k]
    gain = table_ref[OUT_AT : OUT_AT + 1, 0:NOPE]
    for s in range(SEQS):
        scale = lax.rsqrt(total[:, s : s + 1] / D + EPS)
        mixed_ref[s] = (own_ref[s, :, :NOPE] * scale * gain).astype(BF16)
    for s, start in enumerate(starts):

        @pl.when((start > -PROPS) & (start < positions))
        def _(s=s, start=start):
            base = window_base(start, positions)
            pltpu.make_async_copy(patch_ref.at[s], out_hbm.at[s, pl.ds(base, WINDOW), :], sems.at[s]).wait()


def swap(parts, axis):
    return lax.all_to_all(parts, axis, split_axis=0, concat_axis=0, tiled=True)


def body(
    tokens,
    parents,
    lengths,
    accepted,
    in_gain,
    w_query,
    w_latent,
    w_rope_key,
    latent_gain,
    query_gain,
    key_gain,
    w_key_up,
    w_value_up,
    w_out,
    out_gain,
    cache_latent,
    cache_rope,
):
    depth, tall = lax.axis_size("z"), lax.axis_size("y")
    plane = lax.axis_size(PLANE)
    inverse = 10000.0 ** (-(np.arange(LANES) % 16).astype(np.float32) / 16)
    inverse = jnp.asarray(inverse.astype(np.float32).reshape(1, LANES))
    rope_cols = jnp.swapaxes(cache_rope, 1, 2)

    loaded = (
        parents,
        lengths,
        accepted,
        tokens,
        in_gain.reshape(1, -1),
        w_query,
        w_latent,
        w_rope_key.T,
        inverse,
        latent_gain.reshape(1, -1),
        query_gain.reshape(1, -1),
        key_gain.reshape(1, -1),
        out_gain.reshape(1, -1),
        w_out.T,
        rope_cols,
        w_key_up,
        w_value_up,
        cache_latent,
    )
    sent, block_0, block_1, block_2, block_3, table, windows, new_rope, kept = kernel(
        start_body,
        [
            ((tall, CHUNKS, PROPS, LANES), F32),
            *[((BLOCK_ROWS, LANES), F32)] * SEQS,
            ((TABLE_ROWS, LANES), F32),
            ((SEQS, WINDOW, 1024), BF16),
            (rope_cols.shape, BF16),
            (cache_latent.shape, BF16),
        ],
        *[pltpu.with_memory_space_constraint(a, pltpu.HBM) for a in loaded],
        specs=[HBM] * len(loaded),
        out_specs=[VMEM] * 8 + [HBM],
        scratch=[
            (pltpu.SMEM if k < 3 else pltpu.VMEM)(a.shape, a.dtype) for k, a in enumerate(loaded)
        ]
        + [pltpu.SemaphoreType.DMA((len(loaded) + 1,))],
        mebibytes=16,
    )
    reduced = swap(sent, "y")
    leaving = [block_1, block_2, block_3]
    moved = {0: block_0}
    for k in (2, 1, 3):
        moved[k] = lax.ppermute(leaving[k - 1], "y", [(i, (i + k) % SEQS) for i in range(SEQS)])
    blocks = [moved[k] for k in range(SEQS)]
    spread = kernel(relay_body, [((depth, CHUNKS, PROPS, LANES), F32)], reduced)
    gathered = swap(spread, "z")
    query, latent_half = kernel(query_body, [((3, 16, LANES), F32), ((4, PROPS, LANES), F32)], gathered, table)
    latent_both = lax.all_gather(latent_half, "c")
    partial, own, fresh = kernel(
        attend_body,
        [((depth, 3, PROPS, LANES), F32), ((3, PROPS, LANES), F32), ((8, PROPS, LANES), F32)],
        latent_both,
        table,
        query,
        w_key_up,
        w_value_up,
        *blocks,
    )
    partials = swap(partial, "z")
    projected = kernel(merge_body, [((plane, 3, PROPS, LANES), F32)], partials, own, fresh, *blocks)
    projections = swap(projected, PLANE)
    own_columns, squares, fresh_all = kernel(
        gather_body,
        [((SEQS, PROPS, LANES), F32), ((depth, PROPS, LANES), F32), ((SEQS, PROPS, 1024), F32)],
        projections,
    )
    square_parts = swap(squares, "z")
    mixed, new_latent = kernel(
        finish_body,
        [((SEQS, PROPS, NOPE), BF16), (cache_latent.shape, BF16)],
        square_parts,
        own_columns,
        table,
        windows,
        fresh_all,
        kept,
        specs=[VMEM] * 5 + [HBM],
        out_specs=[VMEM, HBM],
        scratch=[pltpu.VMEM((SEQS, WINDOW, 1024), BF16), pltpu.SemaphoreType.DMA((SEQS,))],
        aliases={5: 1},
    )
    return (mixed, new_latent, jnp.swapaxes(new_rope, 1, 2))


def solution(mesh):
    kv, tp = mesh.shape["kv"], mesh.shape["tp"]
    finer = Mesh(mesh.devices.reshape(kv // 4, 4, tp // 2, 2), ("z", "y", "x", "c"))
    tp_axes = ("x", "c")
    placed = (
        P(),
        P(),
        P(),
        P(),
        P(),
        P(KV, tp_axes),
        P(KV, None),
        P(),
        P(),
        P(),
        P(),
        P(None, tp_axes),
        P(None, tp_axes),
        P(tp_axes, KV),
        P(KV),
        P(None, KV, None),
        P(None, KV, None),
    )
    return jax.shard_map(
        body,
        mesh=finer,
        in_specs=placed,
        out_specs=(P(None, None, KV), P(None, KV, None), P(None, KV, None)),
        check_vma=False,
    )
```

profile of v0, /device:TPU:1, one launch (start us, length us, event | category | flops | bytes accessed | tf_op | source)
XLA Modules:
  0.0 110.6 jit_solution(173218766622650052)
XLA Ops:
  0.6 3.9 %shard_map.193 = (f32[4,7,4,128]{3,2,1,0:T(4,128)S(1)}, f32[680,128]{1,0:T(8,128)S(1)}, f32[680,128]{1,0:T(8,128)}, f32[680,128]{1,0:T(8,128)}, f32[680,128]{1,0...) custom-call(s32[4,4]{1,0:T(4,128)} %parents_hbm.1, ...), custom_call_target="tpu_custom_call" | custom-call | flops 2000000 | bytes 1000000 | tf_op jit(solution)/shard_map/pallas_call | solution.py:42
  4.6 9.2 %all_to_all.25.in_ref = f32[4,7,4,128]{3,2,1,0:T(4,128)S(1)} all-to-all(f32[4,7,4,128]{3,2,1,0:T(4,128)S(1)} %get-tuple-element.22), channel_id=1, replica_groups=mesh['z'=16,'y'=4,'x'=4,'c'=2] {'y'}, dimensions={0} | all-to-all | bytes 114688 | tf_op jit(solution)/shard_map/all_to_all | solution.py:532
  13.8 0.0 copy-start
  13.8 0.0 copy-start.1
  13.8 0.7 shard_map.194
  14.6 14.9 %all-to-all-start.1 = ((f32[16,7,4,128]{3,2,1,0:T(4,128)}), f32[16,7,4,128]{3,2,1,0:T(4,128)S(1)}, u32[]{:S(2)}, u32[]{:S(2)}) async-start(f32[16,7,4,128]{3,2,1,0:T(4,128)} %shard_map.194), calls=%async_computation.1 | async-start | bytes 458752 | tf_op jit(solution)/shard_map/all_to_all | solution.py:532
  29.5 2.2 %collective-permute-start = (f32[680,128]{1,0:T(8,128)}, f32[680,128]{1,0:T(8,128)S(1)}, u32[]{:S(2)}, u32[]{:S(2)}) collective-permute-start(f32[680,128]{1,0:T(8,128)} %get-tuple-element.27), channel_id=1, source_target_pairs={{0,8},{8,16},{16,24},{24,0},{1,9},{9,17},{17,25},{25,1},{2,10},{10... | collective-permute-start | bytes 1044488 | tf_op jit(solution)/shard_map/ppermute | solution.py:603
  31.7 3.7 %collective-permute-start.1 = (f32[680,128]{1,0:T(8,128)}, f32[680,128]{1,0:T(8,128)S(1)}, u32[]{:S(2)}, u32[]{:S(2)}) collective-permute-start(f32[680,128]{1,0:T(8,128)} %get-tuple-element.28), channel_id=1, source_target_pairs={{0,16},{8,24},{16,0},{24,8},{1,17},{9,25},{17,1},{25,9},{2,18},{10... | collective-permute-start | bytes 1044488 | tf_op jit(solution)/shard_map/ppermute | solution.py:603
  35.4 2.9 %collective-permute-start.2 = (f32[680,128]{1,0:T(8,128)S(1)}, f32[680,128]{1,0:T(8,128)S(1)}, u32[]{:S(2)}, u32[]{:S(2)}) collective-permute-start(f32[680,128]{1,0:T(8,128)S(1)} %get-tuple-element.29), channel_id=1, source_target_pairs={{0,24},{8,0},{16,8},{24,16},{1,25},{9,1},{17,9},{25,17},{2,26},{10... | collective-permute-start | bytes 1044488 | tf_op jit(solution)/shard_map/ppermute | solution.py:603
  38.3 3.7 %all-to-all-done.1.in_ref = f32[16,7,4,128]{3,2,1,0:T(4,128)S(1)} async-done(((f32[16,7,4,128]{3,2,1,0:T(4,128)}), f32[16,7,4,128]{3,2,1,0:T(4,128)S(1)}, u32[]{:S(2)}, u32[]{:S(2)}) %all-to-all-start.1) | async-done | bytes 229408 | tf_op jit(solution)/shard_map/all_to_all | solution.py:532
  42.0 0.2 shard_map.195
  42.2 7.8 %all-gather = f32[8,4,128]{2,1,0:T(4,128)S(1)} all-gather(f32[4,4,128]{2,1,0:T(4,128)S(1)} %get-tuple-element.24), channel_id=2, replica_groups=mesh['z'=16,'y'=4,'x'=4,'c'=2] {'c'}, dimensions={0}, use_global_device_ids=true | all-gather | bytes 24576 | tf_op jit(solution)/shard_map/all_gather | solution.py:608
  50.0 0.0 collective-permute-done.refs_1_
  50.0 0.0 collective-permute-done.1.refs_2_
  50.0 1.5 %collective-permute-done.2.refs_3_ = f32[680,128]{1,0:T(8,128)S(1)} collective-permute-done((f32[680,128]{1,0:T(8,128)S(1)}, f32[680,128]{1,0:T(8,128)S(1)}, u32[]{:S(2)}, u32[]{:S(2)}) %collective-permute-start.2) | collective-permute-done | bytes 348192 | tf_op jit(solution)/shard_map/ppermute | solution.py:603
  51.6 0.0 copy-done
  51.6 0.0 copy-done.1
  51.6 1.2 %shard_map.196 = (f32[16,3,4,128]{3,2,1,0:T(4,128)S(1)}, f32[3,4,128]{2,1,0:T(4,128)S(1)}, f32[8,4,128]{2,1,0:T(4,128)S(1)}) custom-call(f32[2,4,4,128]{3,2,1,0:T(4,128)S(1)} %bitcast.10, f32[144,128]{1,0:T(8,128)S(1)} %get-tuple-element.23.table_ref, f32[3,16,128]{2,1,0:T(8,128)S(1)} %get-tuple-element.25.query_ref, bf16[1024,256]{1,0:T(8,128)(2,1)S(1)} %copy-done, ...), custom_call_target="tpu_custom_call" | custom-call | flops 2000000 | bytes 1000000 | tf_op jit(solution)/shard_map/pallas_call | solution.py:42
  52.8 22.8 %all_to_all.26.in_ref = f32[16,3,4,128]{3,2,1,0:T(4,128)S(1)} all-to-all(f32[16,3,4,128]{3,2,1,0:T(4,128)S(1)} %get-tuple-element.30), channel_id=1, replica_groups=mesh['z'=16,'y'=4,'x'=4,'c'=2] {'z'}, dimensions={0} | all-to-all | bytes 196608 | tf_op jit(solution)/shard_map/all_to_all | solution.py:532
  75.6 0.5 shard_map.197
  76.1 18.5 %all_to_all.27.in_ref = f32[32,3,4,128]{3,2,1,0:T(4,128)S(1)} all-to-all(f32[32,3,4,128]{3,2,1,0:T(4,128)S(1)} %shard_map.197), channel_id=1, replica_groups=mesh['z'=16,'y'=4,'x'=4,'c'=2] {'y','x','c'}, dimensions={0} | all-to-all | bytes 393216 | tf_op jit(solution)/shard_map/all_to_all | solution.py:532
  94.6 0.1 shard_map.198
  94.7 14.5 %all_to_all.28.in_ref = f32[16,4,128]{2,1,0:T(4,128)S(1)} all-to-all(f32[16,4,128]{2,1,0:T(4,128)S(1)} %get-tuple-element.33), channel_id=1, replica_groups=mesh['z'=16,'y'=4,'x'=4,'c'=2] {'z'}, dimensions={0} | all-to-all | bytes 65536 | tf_op jit(solution)/shard_map/all_to_all | solution.py:532
  109.2 1.4 %shard_map.199 = (bf16[4,4,64]{2,1,0:T(4,128)(2,1)}, bf16[4,128,1024]{2,1,0:T(8,128)(2,1)}) custom-call(f32[16,4,128]{2,1,0:T(4,128)S(1)} %all_to_all.28.in_ref, f32[4,4,128]{2,1,0:T(4,128)S(1)} %get-tuple-element.34.own_ref, f32[144,128]{1,0:T(8,128)S(1)} %get-tuple-element.23.table_ref, ...), custom_call_target="tpu_custom_call", output_to_operand_aliasing={{1}: (5, {})} | custom-call | flops 2000000 | bytes 1000000 | tf_op jit(solution)/shard_map/pallas_call | solution.py:42
Async XLA Ops:
  13.8 37.7 %copy-start = (bf16[1024,256]{1,0:T(8,128)(2,1)S(1)}, bf16[1024,256]{1,0:T(8,128)(2,1)}, u32[]{:S(2)}) copy-start(bf16[1024,256]{1,0:T(8,128)(2,1)} %wk_ref.1) | copy-start | bytes 1572868
  13.8 37.7 %copy-start.1 = (bf16[1024,256]{1,0:T(8,128)(2,1)S(1)}, bf16[1024,256]{1,0:T(8,128)(2,1)}, u32[]{:S(2)}) copy-start(bf16[1024,256]{1,0:T(8,128)(2,1)} %wv_ref.1) | copy-start | bytes 1572868
  14.6 27.4 %all-to-all-start.1 = ((f32[16,7,4,128]{3,2,1,0:T(4,128)}), f32[16,7,4,128]{3,2,1,0:T(4,128)S(1)}, u32[]{:S(2)}, u32[]{:S(2)}) async-start(f32[16,7,4,128]{3,2,1,0:T(4,128)} %shard_map.194), calls=%async_computation.1 | async-start | bytes 458752 | tf_op jit(solution)/shard_map/all_to_all | solution.py:532
  29.5 20.5 %collective-permute-start = (f32[680,128]{1,0:T(8,128)}, f32[680,128]{1,0:T(8,128)S(1)}, u32[]{:S(2)}, u32[]{:S(2)}) collective-permute-start(f32[680,128]{1,0:T(8,128)} %get-tuple-element.27), channel_id=1, source_target_pairs={{0,8},{8,16},{16,24},{24,0},{1,9},{9,17},{17,25},{25,1},{2,10},{10... | collective-permute-start | bytes 1044488 | tf_op jit(solution)/shard_map/ppermute | solution.py:603
  31.7 18.4 %collective-permute-start.1 = (f32[680,128]{1,0:T(8,128)}, f32[680,128]{1,0:T(8,128)S(1)}, u32[]{:S(2)}, u32[]{:S(2)}) collective-permute-start(f32[680,128]{1,0:T(8,128)} %get-tuple-element.28), channel_id=1, source_target_pairs={{0,16},{8,24},{16,0},{24,8},{1,17},{9,25},{17,1},{25,9},{2,18},{10... | collective-permute-start | bytes 1044488 | tf_op jit(solution)/shard_map/ppermute | solution.py:603
  35.4 16.2 %collective-permute-start.2 = (f32[680,128]{1,0:T(8,128)S(1)}, f32[680,128]{1,0:T(8,128)S(1)}, u32[]{:S(2)}, u32[]{:S(2)}) collective-permute-start(f32[680,128]{1,0:T(8,128)S(1)} %get-tuple-element.29), channel_id=1, source_target_pairs={{0,24},{8,0},{16,8},{24,16},{1,25},{9,1},{17,9},{25,17},{2,26},{10... | collective-permute-start | bytes 1044488 | tf_op jit(solution)/shard_map/ppermute | solution.py:603
where the time goes:
time: 111 us
  blocking collectives  72.9 us (66%)
  starting transfers between devices  23.7 us (21%)
  Pallas kernels  8.09 us (7%)
  waiting for transfers between devices  5.2 us (5%)
    all_to_all x4, blocking collectives, swap(): return lax.all_to_all(parts, axis, split_axis=0, concat_axis=0, tiled=True)  65 us
    all_to_all x1, starting transfers between devices, swap(): return lax.all_to_all(parts, axis, split_axis=0, concat_axis=0, tiled=True)  14.9 us
    ppermute x3, starting transfers between devices, body(): lax.ppermute(leaving[k - 1], 'y', [(i, (i + k) % SEQS) for i in range(SEQ...  8.83 us
    pallas_call x7, Pallas kernels, kernel(): pl.pallas_call(body, out_shape=shapes[0] if single else shapes, in_specs=...  8.09 us
    all_gather x1, blocking collectives, body(): latent_both = lax.all_gather(latent_half, 'c')  7.85 us
    all_to_all x1, waiting for transfers between devices, swap(): return lax.all_to_all(parts, axis, split_axis=0, concat_axis=0, tiled=True)  3.65 us
  transfers between devices with their start and end apart: 4, of which 2 were waited for; matrix products, arithmetic and copies ran while one was open for 0% of the time, Pallas kernels for 0%

commit v1 on v0

--- a/solution.py
+++ b/solution.py
@@ -28,6 +28,7 @@
 VMEM = pl.BlockSpec(memory_space=pltpu.VMEM)
 HBM = pl.BlockSpec(memory_space=pltpu.HBM)
 CHUNKS = 7
+PLANE_FIRST, TALL_FIRST = 21, 2
 TURN_AT, SCALE_AT, VALUE_AT, WEIGHT_AT, BLOCK_ROWS = 256, 288, 296, 552, 680
 ROPE_AT, COS_AT, A_AT, B_AT, SEEN_AT, ANCHOR_AT = 0, 4, 8, 12, 16, 32
 QN_AT, QR_AT, KN_AT, KR_AT, OUT_AT, START_AT, LATENT_AT = 33, 34, 35, 36, 37, 38, 40
@@ -181,66 +182,20 @@
     return sum((mask >> j) & 1 for j in range(PROPS))
 
 
-def start_body(
-    parents_hbm,
-    lengths_hbm,
-    accepted_hbm,
-    tok_hbm,
-    gain_hbm,
-    wq_hbm,
-    wl_hbm,
-    wr_hbm,
-    inverse_hbm,
-    lgain_hbm,
-    qgain_hbm,
-    kgain_hbm,
-    ogain_hbm,
-    wo_hbm,
-    rope_hbm,
-    wk_hbm,
-    wv_hbm,
-    cache_hbm,
-    out_ref,
-    block_0,
-    block_1,
-    block_2,
-    block_3,
-    table_ref,
-    window_ref,
-    rope_out_ref,
-    copy_hbm,
-    parents_ref,
-    lengths_ref,
-    accepted_ref,
-    tok_ref,
-    gain_ref,
-    wq_ref,
-    wl_ref,
-    wr_ref,
-    inverse_ref,
-    lgain_ref,
-    qgain_ref,
-    kgain_ref,
-    ogain_ref,
-    wo_ref,
-    rope_ref,
-    wk_ref,
-    wv_ref,
-    cache_ref,
-    sems,
-):
-    sources = (
-        parents_hbm, lengths_hbm, accepted_hbm, tok_hbm, gain_hbm, wq_hbm, wl_hbm, wr_hbm, inverse_hbm,
-        lgain_hbm, qgain_hbm, kgain_hbm, ogain_hbm, wo_hbm, rope_hbm, wk_hbm, wv_hbm, cache_hbm,
-    )
-    targets = (
-        parents_ref, lengths_ref, accepted_ref, tok_ref, gain_ref, wq_ref, wl_ref, wr_ref, inverse_ref,
-        lgain_ref, qgain_ref, kgain_ref, ogain_ref, wo_ref, rope_ref, wk_ref, wv_ref, cache_ref,
-    )
+def load(sources, targets, sems):
     copies = [pltpu.make_async_copy(a, b, sems.at[k]) for k, (a, b) in enumerate(zip(sources, targets))]
     for copy in copies:
         copy.start()
-    for copy in copies[:-4]:
+    return copies
+
+
+def start_body(*refs):
+    sources, refs = refs[:9], refs[9:]
+    (out_ref, *block_refs), refs = refs[:5], refs[5:]
+    targets, (nope_ref, value_ref, sems) = refs[:9], refs[9:]
+    tok_ref, gain_ref, wq_ref, wl_ref, wo_ref, rope_ref, wk_ref, wv_ref, cache_ref = targets
+    copies = load(sources, targets, sems)
+    for copy in copies[:4]:
         copy.wait()
     y = lax.axis_index("y")
     kv = lax.axis_index("z") * lax.axis_size("y") + y
@@ -250,11 +205,10 @@
     base = pl.multiple_of((kv // per) * width, LANES)
     positions = cache_ref.shape[1]
 
-    parts, normed = [], []
+    parts = []
     for s in range(SEQS):
         tok = tok_ref[s].astype(F32)
         scale = lax.rsqrt(jnp.sum(tok * tok, -1, keepdims=True) / D + EPS)
-        normed.append(tok * scale * gain_ref[...])
         piece = tok_ref[s, :, pl.ds(base, width)].astype(F32)
         parts.append(piece * scale * gain_ref[:, pl.ds(base, width)])
     part = jnp.concatenate(parts, 0)
@@ -274,7 +228,56 @@
     ] + [latent[:, LANES * k : LANES * k + LANES] for k in range(half // LANES)]
     for s in range(SEQS):
         for k, chunk in enumerate(chunks):
-            out_ref[s, k] = chunk[4 * s : 4 * s + 4]
+            out_ref[(s - TALL_FIRST) % SEQS, k] = chunk[4 * s : 4 * s + 4]
+
+    for copy in copies[4:]:
+        copy.wait()
+    whole = cache_ref[...].reshape(SEQS * positions, cache_ref.shape[2])
+    nope_ref[...] = matmul(whole, wk_ref[...])
+    value_ref[...] = matmul(whole, wv_ref[...])
+    weights = wo_ref[...].astype(F32)
+    for k, block_ref in enumerate(block_refs):
+        s = lax.rem(y + k, SEQS)
+        at = pl.ds(pl.multiple_of(s * positions, positions), positions)
+        old = rope_ref[s].astype(F32)
+        old_sum = jnp.sum(old * old, 0, keepdims=True)
+        block_ref[TURN_AT : TURN_AT + ROPE] = old
+        for j in range(2):
+            lanes = slice(LANES * j, LANES * j + LANES)
+            flat = nope_ref[at, lanes].T
+            block_ref[lanes] = flat
+            block_ref[VALUE_AT + LANES * j : VALUE_AT + LANES * j + LANES] = value_ref[at, lanes]
+            for i in range(2):
+                dims = flat[NOPE * i : NOPE * i + NOPE]
+                squares = jnp.sum(dims * dims, 0, keepdims=True) + old_sum
+                h = SCALE_AT + 2 * j + i
+                block_ref[h : h + 1] = lax.rsqrt(squares / QK + EPS)
+        block_ref[SCALE_AT + 4 : SCALE_AT + 8] = jnp.zeros((4, LANES), F32)
+        block_ref[WEIGHT_AT : WEIGHT_AT + 64] = weights[:, :LANES]
+        block_ref[WEIGHT_AT + 64 : WEIGHT_AT + 128] = weights[:, LANES:]
+
+
+def aside_body(*refs):
+    sources, refs = refs[:13], refs[13:]
+    (table_ref, window_ref, rope_out_ref, copy_hbm), refs = refs[:4], refs[4:]
+    targets, sems = refs[:13], refs[13]
+    (
+        parents_ref, lengths_ref, accepted_ref, tok_ref, gain_ref, wr_ref,
+        inverse_ref, lgain_ref, qgain_ref, kgain_ref, ogain_ref, rope_ref, cache_ref,
+    ) = targets
+    copies = load(sources, targets, sems)
+    for copy in copies:
+        copy.wait()
+    kept = pltpu.make_async_copy(cache_ref, copy_hbm, sems.at[len(copies)])
+    kept.start()
+    y = lax.axis_index("y")
+    kv = lax.axis_index("z") * lax.axis_size("y") + y
+    positions = cache_ref.shape[1]
+    normed = []
+    for s in range(SEQS):
+        tok = tok_ref[s].astype(F32)
+        scale = lax.rsqrt(jnp.sum(tok * tok, -1, keepdims=True) / D + EPS)
+        normed.append(tok * scale * gain_ref[...])
 
     row = rows_of((16, LANES))
     place = jnp.zeros((16, LANES), F32)
@@ -322,31 +325,6 @@
     table_ref[GAIN_AT + NOPE : GAIN_AT + QK] = jnp.zeros((ROPE, LANES), F32) + tall_gain[:ROPE, 1:2]
     flipped = jnp.concatenate([fresh, jnp.zeros((LANES - 16, LANES), F32)], 0).T[:ROPE]
 
-    for copy in copies[-4:]:
-        copy.wait()
-    kept = pltpu.make_async_copy(cache_ref, copy_hbm, sems.at[len(copies)])
-    kept.start()
-    weights = wo_ref[...].astype(F32)
-    for k, block_ref in enumerate((block_0, block_1, block_2, block_3)):
-        s = lax.rem(y + k, SEQS)
-        block = cache_ref[s]
-        nope = matmul(block, wk_ref[...])
-        value = matmul(block, wv_ref[...])
-        old = rope_ref[s].astype(F32)
-        old_sum = jnp.sum(old * old, 0, keepdims=True)
-        block_ref[TURN_AT : TURN_AT + ROPE] = old
-        for j in range(2):
-            flat = nope[:, LANES * j : LANES * j + LANES].T
-            block_ref[LANES * j : LANES * j + LANES] = flat
-            block_ref[VALUE_AT + LANES * j : VALUE_AT + LANES * j + LANES] = value[:, LANES * j : LANES * j + LANES]
-            for i in range(2):
-                dims = flat[NOPE * i : NOPE * i + NOPE]
-                squares = jnp.sum(dims * dims, 0, keepdims=True) + old_sum
-                h = SCALE_AT + 2 * j + i
-                block_ref[h : h + 1] = lax.rsqrt(squares / QK + EPS)
-        block_ref[SCALE_AT + 4 : SCALE_AT + 8] = jnp.zeros((4, LANES), F32)
-        block_ref[WEIGHT_AT : WEIGHT_AT + 64] = weights[:, :LANES]
-        block_ref[WEIGHT_AT + 64 : WEIGHT_AT + 128] = weights[:, LANES:]
     for s in range(SEQS):
         old = rope_ref[s].astype(F32)
         spot = lanes_of(old.shape)
@@ -399,8 +377,7 @@
     latent_ref[...] = total[3:CHUNKS]
 
 
-def attend_body(latent_ref, table_ref, query_ref, wk_ref, wv_ref, *refs):
-    block_refs, (out_ref, own_ref, fresh_ref) = refs[:SEQS], refs[SEQS:]
+def own_body(latent_ref, table_ref, query_ref, wk_ref, wv_ref, own_ref, fresh_ref):
     query = [query_ref[j].astype(BF16) for j in range(3)]
     pieces = [latent_ref[c, k] for c in range(2) for k in range(4)]
     squares = sum(jnp.sum(piece * piece, -1, keepdims=True) for piece in pieces)
@@ -422,6 +399,11 @@
     own = sum(matmul_t(q, k) for q, k in zip(query, key))
     for j, part in enumerate(attend([own], [value], [table_ref[SEEN_AT : SEEN_AT + 16] > 0.5])):
         own_ref[j] = part
+
+
+def attend_body(table_ref, query_ref, *refs):
+    block_refs, out_ref = refs[:-1], refs[-1]
+    query = [query_ref[j].astype(BF16) for j in range(3)]
     anchor = table_ref[ANCHOR_AT : ANCHOR_AT + 1]
     nope_gain = table_ref[GAIN_AT : GAIN_AT + NOPE]
     rope_gain = table_ref[GAIN_AT + NOPE : GAIN_AT + QK]
@@ -475,22 +457,25 @@
             out_ref[k, j] = part
 
 
-def gather_body(in_ref, own_ref, square_ref, latent_ref):
+def gather_body(whole_ref, own_ref, square_ref, latent_ref):
     y = lax.axis_index("y")
-    peers = in_ref.shape[0] // SEQS
+    size = whole_ref.shape[0]
+    peers = size // SEQS
+    in_ref = [whole_ref.at[(k - PLANE_FIRST) % size] for k in range(size)]
     lane = lanes_of((PROPS, LANES))
     squares = jnp.zeros((PROPS, LANES), F32)
     for s in range(SEQS):
-        first, second = in_ref[peers * s, 0], in_ref[peers * s, 1]
+        first, second = in_ref[peers * s][0], in_ref[peers * s][1]
         for t in range(1, peers):
-            first = first + in_ref[peers * s + t, 0]
-            second = second + in_ref[peers * s + t, 1]
+            first = first + in_ref[peers * s + t][0]
+            second = second + in_ref[peers * s + t][1]
         square = jnp.sum(first * first + second * second, -1, keepdims=True)
-        squares = jnp.where(lane == s, square, squares)
+        squares = squares + jnp.where(lane == PROPS * s + rows_of(lane.shape), square, 0.0)
         picked = jnp.where(y < 2, first, second)
         own_ref[s] = jnp.where(lax.rem(y, 2) == 0, picked, pltpu.roll(picked, NOPE, 1))
         for t in range(peers):
-            latent_ref[s, :, LANES * t : LANES * t + LANES] = in_ref[peers * s + t, 2]
+            latent_ref[s, :, LANES * t : LANES * t + LANES] = in_ref[peers * s + t][2]
+    squares = jnp.sum(squares, 0, keepdims=True)
     for k in range(square_ref.shape[0]):
         square_ref[k] = squares
 
@@ -517,8 +502,10 @@
     for k in range(1, in_ref.shape[0]):
         total = total + in_ref[k]
     gain = table_ref[OUT_AT : OUT_AT + 1, 0:NOPE]
-    for s in range(SEQS):
-        scale = lax.rsqrt(total[:, s : s + 1] / D + EPS)
+    spread = (PROPS, LANES)
+    for s in range(SEQS):
+        square = jnp.where(lanes_of(spread) == PROPS * s + rows_of(spread), total, 0.0)
+        scale = lax.rsqrt(jnp.sum(square, -1, keepdims=True) / D + EPS)
         mixed_ref[s] = (own_ref[s, :, :NOPE] * scale * gain).astype(BF16)
     for s, start in enumerate(starts):
 
@@ -528,8 +515,14 @@
             pltpu.make_async_copy(patch_ref.at[s], out_hbm.at[s, pl.ds(base, WINDOW), :], sems.at[s]).wait()
 
 
-def swap(parts, axis):
-    return lax.all_to_all(parts, axis, split_axis=0, concat_axis=0, tiled=True)
+def swap(parts, axis, first=0):
+    groups = None
+    if first:
+        size = lax.axis_size(axis)
+        groups = [[(first + k) % size for k in range(size)]]
+    return lax.all_to_all(
+        parts, axis, split_axis=0, concat_axis=0, tiled=True, axis_index_groups=groups
+    )
 
 
 def body(
@@ -557,74 +550,72 @@
     inverse = jnp.asarray(inverse.astype(np.float32).reshape(1, LANES))
     rope_cols = jnp.swapaxes(cache_rope, 1, 2)
 
-    loaded = (
-        parents,
-        lengths,
-        accepted,
-        tokens,
-        in_gain.reshape(1, -1),
-        w_query,
-        w_latent,
-        w_rope_key.T,
-        inverse,
-        latent_gain.reshape(1, -1),
-        query_gain.reshape(1, -1),
-        key_gain.reshape(1, -1),
-        out_gain.reshape(1, -1),
-        w_out.T,
-        rope_cols,
-        w_key_up,
-        w_value_up,
-        cache_latent,
-    )
-    sent, block_0, block_1, block_2, block_3, table, windows, new_rope, kept = kernel(
+    in_row = in_gain.reshape(1, -1)
+
+    def from_hbm(body, outs, out_specs, args, extra):
+        args = [pltpu.with_memory_space_constraint(a, pltpu.HBM) for a in args]
+        scratch = [
+            (pltpu.SMEM if a.dtype == jnp.int32 else pltpu.VMEM)(a.shape, a.dtype) for a in args
+        ]
+        return kernel(
+            body,
+            outs,
+            *args,
+            specs=[HBM] * len(args),
+            out_specs=out_specs,
+            scratch=[*scratch, *extra, pltpu.SemaphoreType.DMA((len(args) + 1,))],
+            mebibytes=16,
+        )
+
+    sent, block_0, block_1, block_2, block_3 = from_hbm(
         start_body,
-        [
-            ((tall, CHUNKS, PROPS, LANES), F32),
-            *[((BLOCK_ROWS, LANES), F32)] * SEQS,
-            ((TABLE_ROWS, LANES), F32),
-            ((SEQS, WINDOW, 1024), BF16),
-            (rope_cols.shape, BF16),
-            (cache_latent.shape, BF16),
-        ],
-        *[pltpu.with_memory_space_constraint(a, pltpu.HBM) for a in loaded],
-        specs=[HBM] * len(loaded),
-        out_specs=[VMEM] * 8 + [HBM],
-        scratch=[
-            (pltpu.SMEM if k < 3 else pltpu.VMEM)(a.shape, a.dtype) for k, a in enumerate(loaded)
-        ]
-        + [pltpu.SemaphoreType.DMA((len(loaded) + 1,))],
-        mebibytes=16,
-    )
-    reduced = swap(sent, "y")
+        [((tall, CHUNKS, PROPS, LANES), F32), *[((BLOCK_ROWS, LANES), F32)] * SEQS],
+        [VMEM] * 5,
+        (tokens, in_row, w_query, w_latent, w_out.T, rope_cols, w_key_up, w_value_up, cache_latent),
+        [pltpu.VMEM((SEQS * cache_latent.shape[1], 256), F32)] * 2,
+    )
+    table, windows, new_rope, kept = from_hbm(
+        aside_body,
+        [((TABLE_ROWS, LANES), F32), ((SEQS, WINDOW, 1024), BF16), (rope_cols.shape, BF16), (cache_latent.shape, BF16)],
+        [VMEM] * 3 + [HBM],
+        (
+            parents,
+            lengths,
+            accepted,
+            tokens,
+            in_row,
+            w_rope_key.T,
+            inverse,
+            latent_gain.reshape(1, -1),
+            query_gain.reshape(1, -1),
+            key_gain.reshape(1, -1),
+            out_gain.reshape(1, -1),
+            rope_cols,
+            cache_latent,
+        ),
+        [],
+    )
+    reduced = swap(sent, "y", TALL_FIRST)
     leaving = [block_1, block_2, block_3]
     moved = {0: block_0}
     for k in (2, 1, 3):
         moved[k] = lax.ppermute(leaving[k - 1], "y", [(i, (i + k) % SEQS) for i in range(SEQS)])
     blocks = [moved[k] for k in range(SEQS)]
     spread = kernel(relay_body, [((depth, CHUNKS, PROPS, LANES), F32)], reduced)
-    gathered = swap(spread, "z")
+    gathered = swap(spread, "z", depth // 2)
     query, latent_half = kernel(query_body, [((3, 16, LANES), F32), ((4, PROPS, LANES), F32)], gathered, table)
     latent_both = lax.all_gather(latent_half, "c")
-    partial, own, fresh = kernel(
-        attend_body,
-        [((depth, 3, PROPS, LANES), F32), ((3, PROPS, LANES), F32), ((8, PROPS, LANES), F32)],
-        latent_both,
-        table,
-        query,
-        w_key_up,
-        w_value_up,
-        *blocks,
-    )
-    partials = swap(partial, "z")
+    own, fresh = kernel(
+        own_body, [((3, PROPS, LANES), F32), ((8, PROPS, LANES), F32)], latent_both, table, query, w_key_up, w_value_up
+    )
+    partial = kernel(attend_body, [((depth, 3, PROPS, LANES), F32)], table, query, *blocks)
+    partials = swap(partial, "z", depth // 2)
     projected = kernel(merge_body, [((plane, 3, PROPS, LANES), F32)], partials, own, fresh, *blocks)
-    projections = swap(projected, PLANE)
+    projections = swap(projected, PLANE, PLANE_FIRST)
     own_columns, squares, fresh_all = kernel(
-        gather_body,
-        [((SEQS, PROPS, LANES), F32), ((depth, PROPS, LANES), F32), ((SEQS, PROPS, 1024), F32)],
-        projections,
-    )
-    square_parts = swap(squares, "z")
+        gather_body, [((SEQS, PROPS, LANES), F32), ((depth, 1, LANES), F32), ((SEQS, PROPS, 1024), F32)], projections
+    )
+    square_parts = swap(squares, "z", depth // 2)
     mixed, new_latent = kernel(
         finish_body,
         [((SEQS, PROPS, NOPE), BF16), (cache_latent.shape, BF16)],

time: 111 us -> 99.8 us (0.90)
  the two profiles are of different devices: /device:TPU:1 before, /device:TPU:2 now
where the time goes in v1:
time: 99.8 us; the launch traced here: 99.3 us
  starting transfers between devices  42.4 us (42%)
  blocking collectives  37.1 us (37%)
  Pallas kernels  10.9 us (11%)
  waiting for transfers between devices  8.22 us (8%)
    all_to_all x3, blocking collectives, swap(): lax.all_to_all(parts, axis, split_axis=0, concat_axis=0, tiled=True, axis...  35.3 us
    all_to_all x2, starting transfers between devices, swap(): lax.all_to_all(parts, axis, split_axis=0, concat_axis=0, tiled=True, axis...  30.9 us
    ppermute x3, starting transfers between devices, body(): lax.ppermute(leaving[k - 1], 'y', [(i, (i + k) % SEQS) for i in range(SEQ...  11.5 us
    pallas_call x9, Pallas kernels, kernel(): pl.pallas_call(body, out_shape=shapes[0] if single else shapes, in_specs=...  10.9 us
    ppermute x3, waiting for transfers between devices, body(): lax.ppermute(leaving[k - 1], 'y', [(i, (i + k) % SEQS) for i in range(SEQ...  6.34 us
  transfers between devices with their start and end apart: 5, of which 3 were waited for; matrix products, arithmetic and copies ran while one was open for 0% of the time, Pallas kernels for 4%

profile of v1, /device:TPU:2, one launch (start us, length us, event | category | flops | bytes accessed | tf_op | source)
XLA Modules:
  0.0 99.3 jit_solution(22073464328345864)
XLA Ops:
  0.6 2.8 %shard_map.194 = (f32[4,7,4,128]{3,2,1,0:T(4,128)S(1)}, f32[680,128]{1,0:T(8,128)S(1)}, f32[680,128]{1,0:T(8,128)S(1)}, f32[680,128]{1,0:T(8,128)S(1)}, f32[680,128]{1,0:T(8,128)S(1)}) custom-call(bf16[4,4,4096]{2,1,0:T(4,128)(2,1)} %refs_0_.3, f32[1,4096]{1,0:T(1,128)} %bitcast.14, bf16[64,384]{1,0:T(8,128)(2,1)} %refs_2_.3, bf16[64,1024]{1,0:T(8,128)(2,1)} %refs_3_.3, ...), custom_call_target="tpu_custom_call" | custom-call | flops 2000000 | bytes 1000000 | tf_op jit(solution)/shard_map/pallas_call | solution.py:43
  3.5 8.0 %all_to_all.25.in_ref = f32[4,7,4,128]{3,2,1,0:T(4,128)S(1)} all-to-all(f32[4,7,4,128]{3,2,1,0:T(4,128)S(1)} %get-tuple-element.22), channel_id=1, replica_groups={{16,24,0,8},{17,25,1,9},{18,26,2,10},{19,27,3,11},{20,28,4,12},{21,29,5..., dimensions={0} | all-to-all | bytes 114688 | tf_op jit(solution)/shard_map/all_to_all | solution.py:523
  11.5 0.7 shard_map.195
  12.2 18.9 %all-to-all-start.1 = ((f32[16,7,4,128]{3,2,1,0:T(4,128)}), f32[16,7,4,128]{3,2,1,0:T(4,128)S(1)}, u32[]{:S(2)}, u32[]{:S(2)}) async-start(f32[16,7,4,128]{3,2,1,0:T(4,128)} %shard_map.195), calls=%async_computation.1 | async-start | bytes 458752 | tf_op jit(solution)/shard_map/all_to_all | solution.py:523
  31.1 3.4 %collective-permute-start = (f32[680,128]{1,0:T(8,128)S(1)}, f32[680,128]{1,0:T(8,128)S(1)}, u32[]{:S(2)}, u32[]{:S(2)}) collective-permute-start(f32[680,128]{1,0:T(8,128)S(1)} %get-tuple-element.25), channel_id=1, source_target_pairs={{0,8},{8,16},{16,24},{24,0},{1,9},{9,17},{17,25},{25,1},{2,10},{10... | collective-permute-start | bytes 1044488 | tf_op jit(solution)/shard_map/ppermute | solution.py:602
  34.4 4.6 %collective-permute-start.1 = (f32[680,128]{1,0:T(8,128)S(1)}, f32[680,128]{1,0:T(8,128)S(1)}, u32[]{:S(2)}, u32[]{:S(2)}) collective-permute-start(f32[680,128]{1,0:T(8,128)S(1)} %get-tuple-element.26), channel_id=1, source_target_pairs={{0,16},{8,24},{16,0},{24,8},{1,17},{9,25},{17,1},{25,9},{2,18},{10... | collective-permute-start | bytes 1044488 | tf_op jit(solution)/shard_map/ppermute | solution.py:602
  39.0 3.5 %collective-permute-start.2 = (f32[680,128]{1,0:T(8,128)S(1)}, f32[680,128]{1,0:T(8,128)S(1)}, u32[]{:S(2)}, u32[]{:S(2)}) collective-permute-start(f32[680,128]{1,0:T(8,128)S(1)} %get-tuple-element.27), channel_id=1, source_target_pairs={{0,24},{8,0},{16,8},{24,16},{1,25},{9,1},{17,9},{25,17},{2,26},{10... | collective-permute-start | bytes 1044488 | tf_op jit(solution)/shard_map/ppermute | solution.py:602
  42.6 3.2 %shard_map.193 = (f32[144,128]{1,0:T(8,128)S(1)}, bf16[4,32,1024]{2,1,0:T(8,128)(2,1)S(1)}, bf16[4,32,128]{2,1,0:T(8,128)(2,1)}, bf16[4,128,1024]{2,1,0:T(8,128)(2,1)}) custom-call(s32[4,4]{1,0:T(4,128)} %refs_0_.2, s32[4]{0:T(128)} %refs_1_.1, s32[4]{0:T(128)} %refs_2_.2, bf16[4,4,4096]{2,1,0:T(4,128)(2,1)} %refs_0_.3, f32[1,4096]{1,0:T(1,128)} %bitcast.15, ...), custom_call_target="tpu_custom_call" | custom-call | flops 2000000 | bytes 1000000 | tf_op jit(solution)/shard_map/pallas_call | solution.py:43
  45.8 0.0 all-to-all-done.1.in_ref
  45.8 0.2 shard_map.196
  46.0 0.0 collective-permute-done.refs_1_
  46.0 4.7 %collective-permute-done.1.refs_2_ = f32[680,128]{1,0:T(8,128)S(1)} collective-permute-done((f32[680,128]{1,0:T(8,128)S(1)}, f32[680,128]{1,0:T(8,128)S(1)}, u32[]{:S(2)}, u32[]{:S(2)}) %collective-permute-start.1) | collective-permute-done | bytes 348192 | tf_op jit(solution)/shard_map/ppermute | solution.py:602
  50.7 1.6 %collective-permute-done.2.refs_3_ = f32[680,128]{1,0:T(8,128)S(1)} collective-permute-done((f32[680,128]{1,0:T(8,128)S(1)}, f32[680,128]{1,0:T(8,128)S(1)}, u32[]{:S(2)}, u32[]{:S(2)}) %collective-permute-start.2) | collective-permute-done | bytes 348192 | tf_op jit(solution)/shard_map/ppermute | solution.py:602
  52.3 0.0 copy-start
  52.3 0.0 copy-start.1
  52.3 1.2 %shard_map.197 = f32[16,3,4,128]{3,2,1,0:T(4,128)} custom-call(f32[144,128]{1,0:T(8,128)S(1)} %get-tuple-element.21.table_ref, f32[3,16,128]{2,1,0:T(8,128)S(1)} %get-tuple-element.23.query_ref, f32[680,128]{1,0:T(8,128)S(1)} %get-tuple-element.24.refs_0_, f32[680,128]{1,0:T(8,128)S(1)} %collective-permute-done.refs_1_, ...), custom_call_target="tpu_custom_call" | custom-call | flops 2000000 | bytes 1000000 | tf_op jit(solution)/shard_map/pallas_call | solution.py:43
  53.5 12.0 %all-to-all-start.2 = ((f32[16,3,4,128]{3,2,1,0:T(4,128)}), f32[16,3,4,128]{3,2,1,0:T(4,128)S(1)}, u32[]{:S(2)}, u32[]{:S(2)}) async-start(f32[16,3,4,128]{3,2,1,0:T(4,128)} %shard_map.197), calls=%async_computation.2 | async-start | bytes 196608 | tf_op jit(solution)/shard_map/all_to_all | solution.py:523
  65.6 1.8 %all-gather = f32[8,4,128]{2,1,0:T(4,128)S(1)} all-gather(f32[4,4,128]{2,1,0:T(4,128)S(1)} %get-tuple-element.28), channel_id=2, replica_groups=mesh['z'=16,'y'=4,'x'=4,'c'=2] {'c'}, dimensions={0}, use_global_device_ids=true | all-gather | bytes 24576 | tf_op jit(solution)/shard_map/all_gather | solution.py:607
  67.4 0.0 copy-done
  67.4 0.0 copy-done.1
  67.4 0.7 shard_map.198
  68.1 1.9 %all-to-all-done.2.in_ref = f32[16,3,4,128]{3,2,1,0:T(4,128)S(1)} async-done(((f32[16,3,4,128]{3,2,1,0:T(4,128)}), f32[16,3,4,128]{3,2,1,0:T(4,128)S(1)}, u32[]{:S(2)}, u32[]{:S(2)}) %all-to-all-start.2) | async-done | bytes 98336 | tf_op jit(solution)/shard_map/all_to_all | solution.py:523
  70.0 0.5 shard_map.199
  70.5 13.0 %all_to_all.26.whole_ref = f32[32,3,4,128]{3,2,1,0:T(4,128)S(1)} all-to-all(f32[32,3,4,128]{3,2,1,0:T(4,128)S(1)} %shard_map.199), channel_id=1, replica_groups={{21,22,23,24,25,26,27,28,29,30,31,0,1,2,3,4,5,6,7,8,9,10,11,12,13,14,15..., dimensions={0} | all-to-all | bytes 393216 | tf_op jit(solution)/shard_map/all_to_all | solution.py:523
  83.5 0.1 shard_map.200
  83.6 14.3 %all_to_all.27.in_ref = f32[16,1,128]{2,1,0:T(1,128)S(1)} all-to-all(f32[16,1,128]{2,1,0:T(1,128)S(1)} %get-tuple-element.31), channel_id=1, replica_groups={{256,288,320,352,384,416,448,480,0,32,64,96,128,160,192,224},{257,289,3..., dimensions={0} | all-to-all | bytes 16384 | tf_op jit(solution)/shard_map/all_to_all | solution.py:523
  97.9 1.4 %shard_map.201 = (bf16[4,4,64]{2,1,0:T(4,128)(2,1)}, bf16[4,128,1024]{2,1,0:T(8,128)(2,1)}) custom-call(f32[16,1,128]{2,1,0:T(1,128)S(1)} %all_to_all.27.in_ref, f32[4,4,128]{2,1,0:T(4,128)S(1)} %get-tuple-element.32.own_ref, f32[144,128]{1,0:T(8,128)S(1)} %get-tuple-element.21.table_ref, ...), custom_call_target="tpu_custom_call", output_to_operand_aliasing={{1}: (5, {})} | custom-call | flops 2000000 | bytes 1000000 | tf_op jit(solution)/shard_map/pallas_call | solution.py:43
Async XLA Ops:
  12.2 33.6 %all-to-all-start.1 = ((f32[16,7,4,128]{3,2,1,0:T(4,128)}), f32[16,7,4,128]{3,2,1,0:T(4,128)S(1)}, u32[]{:S(2)}, u32[]{:S(2)}) async-start(f32[16,7,4,128]{3,2,1,0:T(4,128)} %shard_map.195), calls=%async_computation.1 | async-start | bytes 458752 | tf_op jit(solution)/shard_map/all_to_all | solution.py:523
  31.1 14.9 %collective-permute-start = (f32[680,128]{1,0:T(8,128)S(1)}, f32[680,128]{1,0:T(8,128)S(1)}, u32[]{:S(2)}, u32[]{:S(2)}) collective-permute-start(f32[680,128]{1,0:T(8,128)S(1)} %get-tuple-element.25), channel_id=1, source_target_pairs={{0,8},{8,16},{16,24},{24,0},{1,9},{9,17},{17,25},{25,1},{2,10},{10... | collective-permute-start | bytes 1044488 | tf_op jit(solution)/shard_map/ppermute | solution.py:602
  34.4 16.3 %collective-permute-start.1 = (f32[680,128]{1,0:T(8,128)S(1)}, f32[680,128]{1,0:T(8,128)S(1)}, u32[]{:S(2)}, u32[]{:S(2)}) collective-permute-start(f32[680,128]{1,0:T(8,128)S(1)} %get-tuple-element.26), channel_id=1, source_target_pairs={{0,16},{8,24},{16,0},{24,8},{1,17},{9,25},{17,1},{25,9},{2,18},{10... | collective-permute-start | bytes 1044488 | tf_op jit(solution)/shard_map/ppermute | solution.py:602
  39.0 13.3 %collective-permute-start.2 = (f32[680,128]{1,0:T(8,128)S(1)}, f32[680,128]{1,0:T(8,128)S(1)}, u32[]{:S(2)}, u32[]{:S(2)}) collective-permute-start(f32[680,128]{1,0:T(8,128)S(1)} %get-tuple-element.27), channel_id=1, source_target_pairs={{0,24},{8,0},{16,8},{24,16},{1,25},{9,1},{17,9},{25,17},{2,26},{10... | collective-permute-start | bytes 1044488 | tf_op jit(solution)/shard_map/ppermute | solution.py:602
  52.3 15.0 %copy-start = (bf16[1024,256]{1,0:T(8,128)(2,1)S(1)}, bf16[1024,256]{1,0:T(8,128)(2,1)}, u32[]{:S(2)}) copy-start(bf16[1024,256]{1,0:T(8,128)(2,1)} %wk_ref.1) | copy-start | bytes 1572868
  52.3 15.0 %copy-start.1 = (bf16[1024,256]{1,0:T(8,128)(2,1)S(1)}, bf16[1024,256]{1,0:T(8,128)(2,1)}, u32[]{:S(2)}) copy-start(bf16[1024,256]{1,0:T(8,128)(2,1)} %wv_ref.1) | copy-start | bytes 1572868
  53.5 16.4 %all-to-all-start.2 = ((f32[16,3,4,128]{3,2,1,0:T(4,128)}), f32[16,3,4,128]{3,2,1,0:T(4,128)S(1)}, u32[]{:S(2)}, u32[]{:S(2)}) async-start(f32[16,3,4,128]{3,2,1,0:T(4,128)} %shard_map.197), calls=%async_computation.2 | async-start | bytes 196608 | tf_op jit(solution)/shard_map/all_to_all | solution.py:523

commit v2 on v1

--- a/solution.py
+++ b/solution.py
@@ -191,8 +191,8 @@
 
 def start_body(*refs):
     sources, refs = refs[:9], refs[9:]
-    (out_ref, *block_refs), refs = refs[:5], refs[5:]
-    targets, (nope_ref, value_ref, sems) = refs[:9], refs[9:]
+    (out_hbm, *block_refs), refs = refs[:5], refs[5:]
+    targets, (nope_ref, value_ref, out_ref, sems) = refs[:9], refs[9:]
     tok_ref, gain_ref, wq_ref, wl_ref, wo_ref, rope_ref, wk_ref, wv_ref, cache_ref = targets
     copies = load(sources, targets, sems)
     for copy in copies[:4]:
@@ -229,6 +229,8 @@
     for s in range(SEQS):
         for k, chunk in enumerate(chunks):
             out_ref[(s - TALL_FIRST) % SEQS, k] = chunk[4 * s : 4 * s + 4]
+    leaving = pltpu.make_async_copy(out_ref, out_hbm, sems.at[len(copies)])
+    leaving.start()
 
     for copy in copies[4:]:
         copy.wait()
@@ -255,6 +257,7 @@
         block_ref[SCALE_AT + 4 : SCALE_AT + 8] = jnp.zeros((4, LANES), F32)
         block_ref[WEIGHT_AT : WEIGHT_AT + 64] = weights[:, :LANES]
         block_ref[WEIGHT_AT + 64 : WEIGHT_AT + 128] = weights[:, LANES:]
+    leaving.wait()
 
 
 def aside_body(*refs):
@@ -480,7 +483,7 @@
         square_ref[k] = squares
 
 
-def finish_body(in_ref, own_ref, table_ref, window_ref, fresh_ref, copy_hbm, mixed_ref, out_hbm, patch_ref, sems):
+def finish_body(in_ref, own_ref, table_ref, window_ref, fresh_ref, copy_hbm, mixed_hbm, out_hbm, patch_ref, mixed_ref, sems):
     del copy_hbm
     positions = out_hbm.shape[1]
     begun = table_ref[START_AT : START_AT + 1]
@@ -507,12 +510,16 @@
         square = jnp.where(lanes_of(spread) == PROPS * s + rows_of(spread), total, 0.0)
         scale = lax.rsqrt(jnp.sum(square, -1, keepdims=True) / D + EPS)
         mixed_ref[s] = (own_ref[s, :, :NOPE] * scale * gain).astype(BF16)
+    leaving = pltpu.make_async_copy(mixed_ref, mixed_hbm, sems.at[SEQS])
+    leaving.start()
     for s, start in enumerate(starts):
 
         @pl.when((start > -PROPS) & (start < positions))
         def _(s=s, start=start):
             base = window_base(start, positions)
             pltpu.make_async_copy(patch_ref.at[s], out_hbm.at[s, pl.ds(base, WINDOW), :], sems.at[s]).wait()
+
+    leaving.wait()
 
 
 def swap(parts, axis, first=0):
@@ -570,9 +577,10 @@
     sent, block_0, block_1, block_2, block_3 = from_hbm(
         start_body,
         [((tall, CHUNKS, PROPS, LANES), F32), *[((BLOCK_ROWS, LANES), F32)] * SEQS],
-        [VMEM] * 5,
+        [HBM] + [VMEM] * 4,
         (tokens, in_row, w_query, w_latent, w_out.T, rope_cols, w_key_up, w_value_up, cache_latent),
-        [pltpu.VMEM((SEQS * cache_latent.shape[1], 256), F32)] * 2,
+        [pltpu.VMEM((SEQS * cache_latent.shape[1], 256), F32)] * 2
+        + [pltpu.VMEM((tall, CHUNKS, PROPS, LANES), F32)],
     )
     table, windows, new_rope, kept = from_hbm(
         aside_body,
@@ -626,8 +634,12 @@
         fresh_all,
         kept,
         specs=[VMEM] * 5 + [HBM],
-        out_specs=[VMEM, HBM],
-        scratch=[pltpu.VMEM((SEQS, WINDOW, 1024), BF16), pltpu.SemaphoreType.DMA((SEQS,))],
+        out_specs=[HBM, HBM],
+        scratch=[
+            pltpu.VMEM((SEQS, WINDOW, 1024), BF16),
+            pltpu.VMEM((SEQS, PROPS, NOPE), BF16),
+            pltpu.SemaphoreType.DMA((SEQS + 1,)),
+        ],
         aliases={5: 1},
     )
     return (mixed, new_latent, jnp.swapaxes(new_rope, 1, 2))

time: 99.8 us -> 99.3 us (level)
  no operation moved by 1% of the time
where the time goes in v2:
time: 99.3 us; the launch traced here: 98.8 us
  starting transfers between devices  42.4 us (43%)
  blocking collectives  37.1 us (37%)
  Pallas kernels  10.4 us (10%)
  waiting for transfers between devices  8.22 us (8%)
    all_to_all x3, blocking collectives, swap(): lax.all_to_all(parts, axis, split_axis=0, concat_axis=0, tiled=True, axis...  35.3 us
    all_to_all x2, starting transfers between devices, swap(): lax.all_to_all(parts, axis, split_axis=0, concat_axis=0, tiled=True, axis...  30.9 us
    ppermute x3, starting transfers between devices, body(): lax.ppermute(leaving[k - 1], 'y', [(i, (i + k) % SEQS) for i in range(SEQ...  11.5 us
    pallas_call x9, Pallas kernels, kernel(): pl.pallas_call(body, out_shape=shapes[0] if single else shapes, in_specs=...  10.4 us
    ppermute x3, waiting for transfers between devices, body(): lax.ppermute(leaving[k - 1], 'y', [(i, (i + k) % SEQS) for i in range(SEQ...  6.34 us
  transfers between devices with their start and end apart: 5, of which 3 were waited for; matrix products, arithmetic and copies ran while one was open for 0% of the time, Pallas kernels for 4%

profile of v2, /device:TPU:2, one launch (start us, length us, event | category | flops | bytes accessed | tf_op | source)
XLA Modules:
  0.0 98.8 jit_solution(17397682448463286471)
XLA Ops:
  0.6 2.8 %shard_map.194 = (f32[4,7,4,128]{3,2,1,0:T(4,128)S(1)}, f32[680,128]{1,0:T(8,128)S(1)}, f32[680,128]{1,0:T(8,128)S(1)}, f32[680,128]{1,0:T(8,128)S(1)}, f32[680,128]{1,0:T(8,128)S(1)}) custom-call(bf16[4,4,4096]{2,1,0:T(4,128)(2,1)} %refs_0_.3, f32[1,4096]{1,0:T(1,128)} %bitcast.14, bf16[64,384]{1,0:T(8,128)(2,1)} %refs_2_.3, bf16[64,1024]{1,0:T(8,128)(2,1)} %refs_3_.3, ...), custom_call_target="tpu_custom_call" | custom-call | flops 2000000 | bytes 1000000 | tf_op jit(solution)/shard_map/pallas_call | solution.py:43
  3.5 8.0 %all_to_all.25.in_ref = f32[4,7,4,128]{3,2,1,0:T(4,128)S(1)} all-to-all(f32[4,7,4,128]{3,2,1,0:T(4,128)S(1)} %get-tuple-element.22), channel_id=1, replica_groups={{16,24,0,8},{17,25,1,9},{18,26,2,10},{19,27,3,11},{20,28,4,12},{21,29,5..., dimensions={0} | all-to-all | bytes 114688 | tf_op jit(solution)/shard_map/all_to_all | solution.py:530
  11.5 0.7 shard_map.195
  12.2 18.9 %all-to-all-start.1 = ((f32[16,7,4,128]{3,2,1,0:T(4,128)}), f32[16,7,4,128]{3,2,1,0:T(4,128)S(1)}, u32[]{:S(2)}, u32[]{:S(2)}) async-start(f32[16,7,4,128]{3,2,1,0:T(4,128)} %shard_map.195), calls=%async_computation.1 | async-start | bytes 458752 | tf_op jit(solution)/shard_map/all_to_all | solution.py:530
  31.1 3.4 %collective-permute-start = (f32[680,128]{1,0:T(8,128)S(1)}, f32[680,128]{1,0:T(8,128)S(1)}, u32[]{:S(2)}, u32[]{:S(2)}) collective-permute-start(f32[680,128]{1,0:T(8,128)S(1)} %get-tuple-element.25), channel_id=1, source_target_pairs={{0,8},{8,16},{16,24},{24,0},{1,9},{9,17},{17,25},{25,1},{2,10},{10... | collective-permute-start | bytes 1044488 | tf_op jit(solution)/shard_map/ppermute | solution.py:610
  34.4 4.6 %collective-permute-start.1 = (f32[680,128]{1,0:T(8,128)S(1)}, f32[680,128]{1,0:T(8,128)S(1)}, u32[]{:S(2)}, u32[]{:S(2)}) collective-permute-start(f32[680,128]{1,0:T(8,128)S(1)} %get-tuple-element.26), channel_id=1, source_target_pairs={{0,16},{8,24},{16,0},{24,8},{1,17},{9,25},{17,1},{25,9},{2,18},{10... | collective-permute-start | bytes 1044488 | tf_op jit(solution)/shard_map/ppermute | solution.py:610
  39.0 3.5 %collective-permute-start.2 = (f32[680,128]{1,0:T(8,128)S(1)}, f32[680,128]{1,0:T(8,128)S(1)}, u32[]{:S(2)}, u32[]{:S(2)}) collective-permute-start(f32[680,128]{1,0:T(8,128)S(1)} %get-tuple-element.27), channel_id=1, source_target_pairs={{0,24},{8,0},{16,8},{24,16},{1,25},{9,1},{17,9},{25,17},{2,26},{10... | collective-permute-start | bytes 1044488 | tf_op jit(solution)/shard_map/ppermute | solution.py:610
  42.6 3.2 %shard_map.193 = (f32[144,128]{1,0:T(8,128)S(1)}, bf16[4,32,1024]{2,1,0:T(8,128)(2,1)S(1)}, bf16[4,32,128]{2,1,0:T(8,128)(2,1)}, bf16[4,128,1024]{2,1,0:T(8,128)(2,1)}) custom-call(s32[4,4]{1,0:T(4,128)} %refs_0_.2, s32[4]{0:T(128)} %refs_1_.1, s32[4]{0:T(128)} %refs_2_.2, bf16[4,4,4096]{2,1,0:T(4,128)(2,1)} %refs_0_.3, f32[1,4096]{1,0:T(1,128)} %bitcast.15, ...), custom_call_target="tpu_custom_call" | custom-call | flops 2000000 | bytes 1000000 | tf_op jit(solution)/shard_map/pallas_call | solution.py:43
  45.8 0.0 all-to-all-done.1.in_ref
  45.8 0.2 shard_map.196
  46.0 0.0 collective-permute-done.refs_1_
  46.0 4.7 %collective-permute-done.1.refs_2_ = f32[680,128]{1,0:T(8,128)S(1)} collective-permute-done((f32[680,128]{1,0:T(8,128)S(1)}, f32[680,128]{1,0:T(8,128)S(1)}, u32[]{:S(2)}, u32[]{:S(2)}) %collective-permute-start.1) | collective-permute-done | bytes 348192 | tf_op jit(solution)/shard_map/ppermute | solution.py:610
  50.7 1.6 %collective-permute-done.2.refs_3_ = f32[680,128]{1,0:T(8,128)S(1)} collective-permute-done((f32[680,128]{1,0:T(8,128)S(1)}, f32[680,128]{1,0:T(8,128)S(1)}, u32[]{:S(2)}, u32[]{:S(2)}) %collective-permute-start.2) | collective-permute-done | bytes 348192 | tf_op jit(solution)/shard_map/ppermute | solution.py:610
  52.3 0.0 copy-start
  52.3 0.0 copy-start.1
  52.3 1.2 %shard_map.197 = f32[16,3,4,128]{3,2,1,0:T(4,128)} custom-call(f32[144,128]{1,0:T(8,128)S(1)} %get-tuple-element.21.table_ref, f32[3,16,128]{2,1,0:T(8,128)S(1)} %get-tuple-element.23.query_ref, f32[680,128]{1,0:T(8,128)S(1)} %get-tuple-element.24.refs_0_, f32[680,128]{1,0:T(8,128)S(1)} %collective-permute-done.refs_1_, ...), custom_call_target="tpu_custom_call" | custom-call | flops 2000000 | bytes 1000000 | tf_op jit(solution)/shard_map/pallas_call | solution.py:43
  53.5 12.0 %all-to-all-start.2 = ((f32[16,3,4,128]{3,2,1,0:T(4,128)}), f32[16,3,4,128]{3,2,1,0:T(4,128)S(1)}, u32[]{:S(2)}, u32[]{:S(2)}) async-start(f32[16,3,4,128]{3,2,1,0:T(4,128)} %shard_map.197), calls=%async_computation.2 | async-start | bytes 196608 | tf_op jit(solution)/shard_map/all_to_all | solution.py:530
  65.6 1.8 %all-gather = f32[8,4,128]{2,1,0:T(4,128)S(1)} all-gather(f32[4,4,128]{2,1,0:T(4,128)S(1)} %get-tuple-element.28), channel_id=2, replica_groups=mesh['z'=16,'y'=4,'x'=4,'c'=2] {'c'}, dimensions={0}, use_global_device_ids=true | all-gather | bytes 24576 | tf_op jit(solution)/shard_map/all_gather | solution.py:615
  67.4 0.0 copy-done
  67.4 0.0 copy-done.1
  67.4 0.7 shard_map.198
  68.1 1.9 %all-to-all-done.2.in_ref = f32[16,3,4,128]{3,2,1,0:T(4,128)S(1)} async-done(((f32[16,3,4,128]{3,2,1,0:T(4,128)}), f32[16,3,4,128]{3,2,1,0:T(4,128)S(1)}, u32[]{:S(2)}, u32[]{:S(2)}) %all-to-all-start.2) | async-done | bytes 98336 | tf_op jit(solution)/shard_map/all_to_all | solution.py:530
  70.0 0.5 shard_map.199
  70.5 13.0 %all_to_all.26.whole_ref = f32[32,3,4,128]{3,2,1,0:T(4,128)S(1)} all-to-all(f32[32,3,4,128]{3,2,1,0:T(4,128)S(1)} %shard_map.199), channel_id=1, replica_groups={{21,22,23,24,25,26,27,28,29,30,31,0,1,2,3,4,5,6,7,8,9,10,11,12,13,14,15..., dimensions={0} | all-to-all | bytes 393216 | tf_op jit(solution)/shard_map/all_to_all | solution.py:530
  83.5 0.1 shard_map.200
  83.6 14.3 %all_to_all.27.in_ref = f32[16,1,128]{2,1,0:T(1,128)S(1)} all-to-all(f32[16,1,128]{2,1,0:T(1,128)S(1)} %get-tuple-element.31), channel_id=1, replica_groups={{256,288,320,352,384,416,448,480,0,32,64,96,128,160,192,224},{257,289,3..., dimensions={0} | all-to-all | bytes 16384 | tf_op jit(solution)/shard_map/all_to_all | solution.py:530
  97.9 0.9 shard_map.201
Async XLA Ops:
  12.2 33.6 %all-to-all-start.1 = ((f32[16,7,4,128]{3,2,1,0:T(4,128)}), f32[16,7,4,128]{3,2,1,0:T(4,128)S(1)}, u32[]{:S(2)}, u32[]{:S(2)}) async-start(f32[16,7,4,128]{3,2,1,0:T(4,128)} %shard_map.195), calls=%async_computation.1 | async-start | bytes 458752 | tf_op jit(solution)/shard_map/all_to_all | solution.py:530
  31.1 14.9 %collective-permute-start = (f32[680,128]{1,0:T(8,128)S(1)}, f32[680,128]{1,0:T(8,128)S(1)}, u32[]{:S(2)}, u32[]{:S(2)}) collective-permute-start(f32[680,128]{1,0:T(8,128)S(1)} %get-tuple-element.25), channel_id=1, source_target_pairs={{0,8},{8,16},{16,24},{24,0},{1,9},{9,17},{17,25},{25,1},{2,10},{10... | collective-permute-start | bytes 1044488 | tf_op jit(solution)/shard_map/ppermute | solution.py:610
  34.4 16.3 %collective-permute-start.1 = (f32[680,128]{1,0:T(8,128)S(1)}, f32[680,128]{1,0:T(8,128)S(1)}, u32[]{:S(2)}, u32[]{:S(2)}) collective-permute-start(f32[680,128]{1,0:T(8,128)S(1)} %get-tuple-element.26), channel_id=1, source_target_pairs={{0,16},{8,24},{16,0},{24,8},{1,17},{9,25},{17,1},{25,9},{2,18},{10... | collective-permute-start | bytes 1044488 | tf_op jit(solution)/shard_map/ppermute | solution.py:610
  39.0 13.3 %collective-permute-start.2 = (f32[680,128]{1,0:T(8,128)S(1)}, f32[680,128]{1,0:T(8,128)S(1)}, u32[]{:S(2)}, u32[]{:S(2)}) collective-permute-start(f32[680,128]{1,0:T(8,128)S(1)} %get-tuple-element.27), channel_id=1, source_target_pairs={{0,24},{8,0},{16,8},{24,16},{1,25},{9,1},{17,9},{25,17},{2,26},{10... | collective-permute-start | bytes 1044488 | tf_op jit(solution)/shard_map/ppermute | solution.py:610
  52.3 15.0 %copy-start = (bf16[1024,256]{1,0:T(8,128)(2,1)S(1)}, bf16[1024,256]{1,0:T(8,128)(2,1)}, u32[]{:S(2)}) copy-start(bf16[1024,256]{1,0:T(8,128)(2,1)} %wk_ref.1) | copy-start | bytes 1572868
  52.3 15.0 %copy-start.1 = (bf16[1024,256]{1,0:T(8,128)(2,1)S(1)}, bf16[1024,256]{1,0:T(8,128)(2,1)}, u32[]{:S(2)}) copy-start(bf16[1024,256]{1,0:T(8,128)(2,1)} %wv_ref.1) | copy-start | bytes 1572868
  53.5 16.4 %all-to-all-start.2 = ((f32[16,3,4,128]{3,2,1,0:T(4,128)}), f32[16,3,4,128]{3,2,1,0:T(4,128)S(1)}, u32[]{:S(2)}, u32[]{:S(2)}) async-start(f32[16,3,4,128]{3,2,1,0:T(4,128)} %shard_map.197), calls=%async_computation.2 | async-start | bytes 196608 | tf_op jit(solution)/shard_map/all_to_all | solution.py:530

commit v3 on v2

--- a/solution.py
+++ b/solution.py
@@ -522,11 +522,14 @@
     leaving.wait()
 
 
-def swap(parts, axis, first=0):
+def swap(parts, axis, first=0, apart=False):
     groups = None
     if first:
         size = lax.axis_size(axis)
-        groups = [[(first + k) % size for k in range(size)]]
+        order = range(size)
+        if apart:
+            order = [k // 2 + (k % 2) * (size // 2) for k in range(size)]
+        groups = [[(first + k) % size for k in order]]
     return lax.all_to_all(
         parts, axis, split_axis=0, concat_axis=0, tiled=True, axis_index_groups=groups
     )
@@ -610,20 +613,20 @@
         moved[k] = lax.ppermute(leaving[k - 1], "y", [(i, (i + k) % SEQS) for i in range(SEQS)])
     blocks = [moved[k] for k in range(SEQS)]
     spread = kernel(relay_body, [((depth, CHUNKS, PROPS, LANES), F32)], reduced)
-    gathered = swap(spread, "z", depth // 2)
+    gathered = swap(spread, "z", depth // 2 + 1)
     query, latent_half = kernel(query_body, [((3, 16, LANES), F32), ((4, PROPS, LANES), F32)], gathered, table)
     latent_both = lax.all_gather(latent_half, "c")
     own, fresh = kernel(
         own_body, [((3, PROPS, LANES), F32), ((8, PROPS, LANES), F32)], latent_both, table, query, w_key_up, w_value_up
     )
     partial = kernel(attend_body, [((depth, 3, PROPS, LANES), F32)], table, query, *blocks)
-    partials = swap(partial, "z", depth // 2)
+    partials = swap(partial, "z", depth // 2 + 1, apart=True)
     projected = kernel(merge_body, [((plane, 3, PROPS, LANES), F32)], partials, own, fresh, *blocks)
     projections = swap(projected, PLANE, PLANE_FIRST)
     own_columns, squares, fresh_all = kernel(
         gather_body, [((SEQS, PROPS, LANES), F32), ((depth, 1, LANES), F32), ((SEQS, PROPS, 1024), F32)], projections
     )
-    square_parts = swap(squares, "z", depth // 2)
+    square_parts = swap(squares, "z", depth // 2 + 1)
     mixed, new_latent = kernel(
         finish_body,
         [((SEQS, PROPS, NOPE), BF16), (cache_latent.shape, BF16)],

time: 99.3 us -> 100 us (level)
  no operation moved by 1% of the time
where the time goes in v3:
time: 100 us; the launch traced here: 99.6 us
  starting transfers between devices  41.5 us (42%)
  blocking collectives  37.9 us (38%)
  Pallas kernels  10.4 us (10%)
  waiting for transfers between devices  9.06 us (9%)
    all_to_all x3, blocking collectives, swap(): lax.all_to_all(parts, axis, split_axis=0, concat_axis=0, tiled=True, axis...  36.1 us
    all_to_all x2, starting transfers between devices, swap(): lax.all_to_all(parts, axis, split_axis=0, concat_axis=0, tiled=True, axis...  30 us
    ppermute x3, starting transfers between devices, body(): lax.ppermute(leaving[k - 1], 'y', [(i, (i + k) % SEQS) for i in range(SEQ...  11.5 us
    pallas_call x9, Pallas kernels, kernel(): pl.pallas_call(body, out_shape=shapes[0] if single else shapes, in_specs=...  10.4 us
    ppermute x3, waiting for transfers between devices, body(): lax.ppermute(leaving[k - 1], 'y', [(i, (i + k) % SEQS) for i in range(SEQ...  6.34 us
    all_to_all x2, waiting for transfers between devices, swap(): lax.all_to_all(parts, axis, split_axis=0, concat_axis=0, tiled=True, axis...  2.71 us
  transfers between devices with their start and end apart: 5, of which 3 were waited for; matrix products, arithmetic and copies ran while one was open for 0% of the time, Pallas kernels for 4%

profile of v3, /device:TPU:2, one launch (start us, length us, event | category | flops | bytes accessed | tf_op | source)
XLA Modules:
  0.0 99.6 jit_solution(13753384702794450667)
XLA Ops:
  0.6 2.8 %shard_map.194 = (f32[4,7,4,128]{3,2,1,0:T(4,128)S(1)}, f32[680,128]{1,0:T(8,128)S(1)}, f32[680,128]{1,0:T(8,128)S(1)}, f32[680,128]{1,0:T(8,128)S(1)}, f32[680,128]{1,0:T(8,128)S(1)}) custom-call(bf16[4,4,4096]{2,1,0:T(4,128)(2,1)} %refs_0_.3, f32[1,4096]{1,0:T(1,128)} %bitcast.14, bf16[64,384]{1,0:T(8,128)(2,1)} %refs_2_.3, bf16[64,1024]{1,0:T(8,128)(2,1)} %refs_3_.3, ...), custom_call_target="tpu_custom_call" | custom-call | flops 2000000 | bytes 1000000 | tf_op jit(solution)/shard_map/pallas_call | solution.py:43
  3.5 8.0 %all_to_all.25.in_ref = f32[4,7,4,128]{3,2,1,0:T(4,128)S(1)} all-to-all(f32[4,7,4,128]{3,2,1,0:T(4,128)S(1)} %get-tuple-element.22), channel_id=1, replica_groups={{16,24,0,8},{17,25,1,9},{18,26,2,10},{19,27,3,11},{20,28,4,12},{21,29,5..., dimensions={0} | all-to-all | bytes 114688 | tf_op jit(solution)/shard_map/all_to_all | solution.py:533
  11.5 0.7 shard_map.195
  12.2 18.0 %all-to-all-start.1 = ((f32[16,7,4,128]{3,2,1,0:T(4,128)}), f32[16,7,4,128]{3,2,1,0:T(4,128)S(1)}, u32[]{:S(2)}, u32[]{:S(2)}) async-start(f32[16,7,4,128]{3,2,1,0:T(4,128)} %shard_map.195), calls=%async_computation.1 | async-start | bytes 458752 | tf_op jit(solution)/shard_map/all_to_all | solution.py:533
  30.2 3.4 %collective-permute-start = (f32[680,128]{1,0:T(8,128)S(1)}, f32[680,128]{1,0:T(8,128)S(1)}, u32[]{:S(2)}, u32[]{:S(2)}) collective-permute-start(f32[680,128]{1,0:T(8,128)S(1)} %get-tuple-element.25), channel_id=1, source_target_pairs={{0,8},{8,16},{16,24},{24,0},{1,9},{9,17},{17,25},{25,1},{2,10},{10... | collective-permute-start | bytes 1044488 | tf_op jit(solution)/shard_map/ppermute | solution.py:613
  33.5 4.6 %collective-permute-start.1 = (f32[680,128]{1,0:T(8,128)S(1)}, f32[680,128]{1,0:T(8,128)S(1)}, u32[]{:S(2)}, u32[]{:S(2)}) collective-permute-start(f32[680,128]{1,0:T(8,128)S(1)} %get-tuple-element.26), channel_id=1, source_target_pairs={{0,16},{8,24},{16,0},{24,8},{1,17},{9,25},{17,1},{25,9},{2,18},{10... | collective-permute-start | bytes 1044488 | tf_op jit(solution)/shard_map/ppermute | solution.py:613
  38.1 3.5 %collective-permute-start.2 = (f32[680,128]{1,0:T(8,128)S(1)}, f32[680,128]{1,0:T(8,128)S(1)}, u32[]{:S(2)}, u32[]{:S(2)}) collective-permute-start(f32[680,128]{1,0:T(8,128)S(1)} %get-tuple-element.27), channel_id=1, source_target_pairs={{0,24},{8,0},{16,8},{24,16},{1,25},{9,1},{17,9},{25,17},{2,26},{10... | collective-permute-start | bytes 1044488 | tf_op jit(solution)/shard_map/ppermute | solution.py:613
  41.7 3.2 %shard_map.193 = (f32[144,128]{1,0:T(8,128)S(1)}, bf16[4,32,1024]{2,1,0:T(8,128)(2,1)S(1)}, bf16[4,32,128]{2,1,0:T(8,128)(2,1)}, bf16[4,128,1024]{2,1,0:T(8,128)(2,1)}) custom-call(s32[4,4]{1,0:T(4,128)} %refs_0_.2, s32[4]{0:T(128)} %refs_1_.1, s32[4]{0:T(128)} %refs_2_.2, bf16[4,4,4096]{2,1,0:T(4,128)(2,1)} %refs_0_.3, f32[1,4096]{1,0:T(1,128)} %bitcast.15, ...), custom_call_target="tpu_custom_call" | custom-call | flops 2000000 | bytes 1000000 | tf_op jit(solution)/shard_map/pallas_call | solution.py:43
  44.9 0.0 all-to-all-done.1.in_ref
  44.9 0.2 shard_map.196
  45.1 0.0 collective-permute-done.refs_1_
  45.1 4.7 %collective-permute-done.1.refs_2_ = f32[680,128]{1,0:T(8,128)S(1)} collective-permute-done((f32[680,128]{1,0:T(8,128)S(1)}, f32[680,128]{1,0:T(8,128)S(1)}, u32[]{:S(2)}, u32[]{:S(2)}) %collective-permute-start.1) | collective-permute-done | bytes 348192 | tf_op jit(solution)/shard_map/ppermute | solution.py:613
  49.8 1.6 %collective-permute-done.2.refs_3_ = f32[680,128]{1,0:T(8,128)S(1)} collective-permute-done((f32[680,128]{1,0:T(8,128)S(1)}, f32[680,128]{1,0:T(8,128)S(1)}, u32[]{:S(2)}, u32[]{:S(2)}) %collective-permute-start.2) | collective-permute-done | bytes 348192 | tf_op jit(solution)/shard_map/ppermute | solution.py:613
  51.4 0.0 copy-start
  51.4 0.0 copy-start.1
  51.4 1.2 %shard_map.197 = f32[16,3,4,128]{3,2,1,0:T(4,128)} custom-call(f32[144,128]{1,0:T(8,128)S(1)} %get-tuple-element.21.table_ref, f32[3,16,128]{2,1,0:T(8,128)S(1)} %get-tuple-element.23.query_ref, f32[680,128]{1,0:T(8,128)S(1)} %get-tuple-element.24.refs_0_, f32[680,128]{1,0:T(8,128)S(1)} %collective-permute-done.refs_1_, ...), custom_call_target="tpu_custom_call" | custom-call | flops 2000000 | bytes 1000000 | tf_op jit(solution)/shard_map/pallas_call | solution.py:43
  52.6 12.0 %all-to-all-start.2 = ((f32[16,3,4,128]{3,2,1,0:T(4,128)}), f32[16,3,4,128]{3,2,1,0:T(4,128)S(1)}, u32[]{:S(2)}, u32[]{:S(2)}) async-start(f32[16,3,4,128]{3,2,1,0:T(4,128)} %shard_map.197), calls=%async_computation.2 | async-start | bytes 196608 | tf_op jit(solution)/shard_map/all_to_all | solution.py:533
  64.7 1.8 %all-gather = f32[8,4,128]{2,1,0:T(4,128)S(1)} all-gather(f32[4,4,128]{2,1,0:T(4,128)S(1)} %get-tuple-element.28), channel_id=2, replica_groups=mesh['z'=16,'y'=4,'x'=4,'c'=2] {'c'}, dimensions={0}, use_global_device_ids=true | all-gather | bytes 24576 | tf_op jit(solution)/shard_map/all_gather | solution.py:618
  66.5 0.0 copy-done
  66.5 0.0 copy-done.1
  66.5 0.7 shard_map.198
  67.2 2.7 %all-to-all-done.2.in_ref = f32[16,3,4,128]{3,2,1,0:T(4,128)S(1)} async-done(((f32[16,3,4,128]{3,2,1,0:T(4,128)}), f32[16,3,4,128]{3,2,1,0:T(4,128)S(1)}, u32[]{:S(2)}, u32[]{:S(2)}) %all-to-all-start.2) | async-done | bytes 98336 | tf_op jit(solution)/shard_map/all_to_all | solution.py:533
  69.9 0.5 shard_map.199
  70.5 13.0 %all_to_all.26.whole_ref = f32[32,3,4,128]{3,2,1,0:T(4,128)S(1)} all-to-all(f32[32,3,4,128]{3,2,1,0:T(4,128)S(1)} %shard_map.199), channel_id=1, replica_groups={{21,22,23,24,25,26,27,28,29,30,31,0,1,2,3,4,5,6,7,8,9,10,11,12,13,14,15..., dimensions={0} | all-to-all | bytes 393216 | tf_op jit(solution)/shard_map/all_to_all | solution.py:533
  83.4 0.1 shard_map.200
  83.5 15.2 %all_to_all.27.in_ref = f32[16,1,128]{2,1,0:T(1,128)S(1)} all-to-all(f32[16,1,128]{2,1,0:T(1,128)S(1)} %get-tuple-element.31), channel_id=1, replica_groups={{288,320,352,384,416,448,480,0,32,64,96,128,160,192,224,256},{289,321,3..., dimensions={0} | all-to-all | bytes 16384 | tf_op jit(solution)/shard_map/all_to_all | solution.py:533
  98.7 0.9 shard_map.201
Async XLA Ops:
  12.2 32.7 %all-to-all-start.1 = ((f32[16,7,4,128]{3,2,1,0:T(4,128)}), f32[16,7,4,128]{3,2,1,0:T(4,128)S(1)}, u32[]{:S(2)}, u32[]{:S(2)}) async-start(f32[16,7,4,128]{3,2,1,0:T(4,128)} %shard_map.195), calls=%async_computation.1 | async-start | bytes 458752 | tf_op jit(solution)/shard_map/all_to_all | solution.py:533
  30.2 14.9 %collective-permute-start = (f32[680,128]{1,0:T(8,128)S(1)}, f32[680,128]{1,0:T(8,128)S(1)}, u32[]{:S(2)}, u32[]{:S(2)}) collective-permute-start(f32[680,128]{1,0:T(8,128)S(1)} %get-tuple-element.25), channel_id=1, source_target_pairs={{0,8},{8,16},{16,24},{24,0},{1,9},{9,17},{17,25},{25,1},{2,10},{10... | collective-permute-start | bytes 1044488 | tf_op jit(solution)/shard_map/ppermute | solution.py:613
  33.5 16.3 %collective-permute-start.1 = (f32[680,128]{1,0:T(8,128)S(1)}, f32[680,128]{1,0:T(8,128)S(1)}, u32[]{:S(2)}, u32[]{:S(2)}) collective-permute-start(f32[680,128]{1,0:T(8,128)S(1)} %get-tuple-element.26), channel_id=1, source_target_pairs={{0,16},{8,24},{16,0},{24,8},{1,17},{9,25},{17,1},{25,9},{2,18},{10... | collective-permute-start | bytes 1044488 | tf_op jit(solution)/shard_map/ppermute | solution.py:613
  38.1 13.3 %collective-permute-start.2 = (f32[680,128]{1,0:T(8,128)S(1)}, f32[680,128]{1,0:T(8,128)S(1)}, u32[]{:S(2)}, u32[]{:S(2)}) collective-permute-start(f32[680,128]{1,0:T(8,128)S(1)} %get-tuple-element.27), channel_id=1, source_target_pairs={{0,24},{8,0},{16,8},{24,16},{1,25},{9,1},{17,9},{25,17},{2,26},{10... | collective-permute-start | bytes 1044488 | tf_op jit(solution)/shard_map/ppermute | solution.py:613
  51.4 15.0 %copy-start = (bf16[1024,256]{1,0:T(8,128)(2,1)S(1)}, bf16[1024,256]{1,0:T(8,128)(2,1)}, u32[]{:S(2)}) copy-start(bf16[1024,256]{1,0:T(8,128)(2,1)} %wk_ref.1) | copy-start | bytes 1572868
  51.4 15.0 %copy-start.1 = (bf16[1024,256]{1,0:T(8,128)(2,1)S(1)}, bf16[1024,256]{1,0:T(8,128)(2,1)}, u32[]{:S(2)}) copy-start(bf16[1024,256]{1,0:T(8,128)(2,1)} %wv_ref.1) | copy-start | bytes 1572868
  52.6 17.3 %all-to-all-start.2 = ((f32[16,3,4,128]{3,2,1,0:T(4,128)}), f32[16,3,4,128]{3,2,1,0:T(4,128)S(1)}, u32[]{:S(2)}, u32[]{:S(2)}) async-start(f32[16,3,4,128]{3,2,1,0:T(4,128)} %shard_map.197), calls=%async_computation.2 | async-start | bytes 196608 | tf_op jit(solution)/shard_map/all_to_all | solution.py:533
